TPU v7x, 32 devices: a whole 2x2x4 slice. The times are simulated.
32 devices in a mesh: ep: 4 (over y, x), tp: 8 (over z, core).
Axes of the slice: x: 2, y: 2, z: 4, core: 2. Of those that a mesh axis runs over, the one named last changes fastest.
Arguments:
- mixer_in: bfloat16 [8192, 2048], P(('ep', 'tp')), may hold values from -6 to 6
- pre_gain: float32 [2048], replicated, may hold values from 0.1 to 1.9
- glu_value: bfloat16 [2048, 1024], P(None, 'tp'), may hold values from -0.125 to 0.125
- glu_gate: bfloat16 [2048, 1024], P(None, 'tp'), may hold values from -0.125 to 0.125
- conv_kernel: float32 [31, 1024], replicated, may hold values from -1 to 1
- chan_gain: float32 [1024], replicated, may hold values from 0.1 to 1.9
- out_weight: bfloat16 [1024, 2048], P(None, 'tp'), may hold values from -0.1875 to 0.1875
- mix_gain: float32 [2048], replicated, may hold values from 0.1 to 1.9
- expert_in: bfloat16 [1024, 2048], P(('ep', 'tp')), may hold values from -6 to 6
- ffn_gain: float32 [2048], replicated, may hold values from 0.1 to 1.9
- routing: int32 [1024, 2], P(('ep', 'tp')), may hold values from 0 to 7, all different within a row; in each aligned block of 32 rows (0 to 31, 32 to 63, ...) at most 12 rows name the same one
- route_weight: float32 [1024, 2], P(('ep', 'tp')), may hold values from 0.1 to 1
- gate_proj: bfloat16 [8, 2048, 4096], P('ep', None, 'tp'), may hold values from -0.375 to 0.375
- up_proj: bfloat16 [8, 2048, 4096], P('ep', None, 'tp'), may hold values from -0.375 to 0.375
- down_proj: bfloat16 [8, 4096, 2048], P('ep', 'tp'), may hold values from -0.09375 to 0.09375
- expert_gain: float32 [2048], replicated, may hold values from 0.1 to 1.9
Outputs:
- mixed: bfloat16 [8192, 2048], P(('ep', 'tp'))
- routed: bfloat16 [1024, 2048], P(('ep', 'tp'))
Inputs may be any that keep to these rules, and one draw needn't show every extreme that they name: `routing`: each row names 2 different experts; in each aligned block of 32 rows (the rows of one device) no expert is named more than 12 times.
All inputs are finite; a program needn't handle non-finite values.
Results may differ from a plain program's by a relative error of at most 0.02.
Values may be sent and summed in bfloat16 or wider, within the bound.
A program may use at most 128 MiB of HBM per device.

v0:
```python
import functools

import jax
import jax.numpy as jnp
from jax import lax
from jax.experimental import pallas as pl
from jax.experimental.pallas import tpu as pltpu
from jax.sharding import PartitionSpec as P

RMS_EPSILON = 1e-06
LAYER_EPSILON = 1e-05
CLAMP_LIMIT = 7.0
SWISH_ALPHA = 1.702


def passed_along(value, axis, steps):
    count = lax.axis_size(axis)
    initial, last = (max(0, -steps), min(count, count - steps))
    return lax.ppermute(value, axis, [(source, source + steps) for source in range(initial, last)])


def rms_scale(values, gain_row):
    values = values.astype(jnp.float32)
    return (
        values
        * lax.rsqrt(jnp.mean(values * values, axis=-1, keepdims=True) + RMS_EPSILON)
        * gain_row
    )


def columns(ref, owner, width, rows):
    if len(ref.shape) == 3:
        return ref.at[owner, rows, :]
    return ref.at[rows, pl.ds(pl.multiple_of(owner * width, width), width)]


def exchange_kernel(
    groups_ep,
    groups_tp,
    capacity,
    inside,
    outgoing,
    mixer_in,
    pre_gain,
    conv_kernel,
    chan_gain,
    mix_gain,
    value_own,
    gate_own,
    out_own,
    gate_hbm,
    up_hbm,
    down_hbm,
    *rest,
):
    if inside:
        mixed, returned, value_full, gate_full, out_full, *rest = rest
        normed, padded, conv, act, projected, *rest = rest
    else:
        value_full, gate_full, out_full, returned, *rest = rest
    (
    rows_all,
    hidden,
    partial,
    pair_in,
    ring_in,
    back_out,
    back_in,
    gate_vmem,
    up_vmem,
    down_vmem,
    load_sem,
    stage_sem,
    send_h,
    recv_h,
    own_sem,
    send_a,
    recv_a,
    send_r,
    recv_r,
    send_rp,
    recv_rp,
    send_w1,
    recv_w1,
    send_w2,
    recv_w2,
    send_wp,
    recv_wp,
    send_p,
    recv_p,
    send_z,
    recv_z,
    send_b,
    recv_b,
    ) = rest
    q = lax.axis_index("ep")
    t = lax.axis_index("tp")
    chips = groups_tp // 2
    z, core = t // 2, t % 2
    partner = z * 2 + 1 - core
    chunk, width = rows_all.shape[1], rows_all.shape[2]
    slots = chunk // groups_ep
    local_experts, _, units = gate_vmem.shape

    def remote(src, dst, send, recv, ep, tp):
        return pltpu.make_async_remote_copy(
            src_ref=src,
            dst_ref=dst,
            send_sem=send,
            recv_sem=recv,
            device_id=(ep, tp),
            device_id_type=pl.DeviceIdType.MESH,
        )

    barrier = pltpu.get_barrier_semaphore()
    others = [(lax.rem(q + i, groups_ep), t) for i in range(1, groups_ep)]
    others += [(q, lax.rem(z + i, chips) * 2 + core) for i in range(1, chips)]
    others += [(q, partner)]
    me, devices = q * groups_tp + t, groups_ep * groups_tp
    after, ahead = lax.rem(me + 1, devices), lax.rem(me + devices - 1, devices)
    others += [(n // groups_tp, lax.rem(n, groups_tp)) for n in (after, ahead)]

    def greet(ep, tp):
        pl.semaphore_signal(
            barrier, inc=1, device_id=(ep, tp), device_id_type=pl.DeviceIdType.MESH
        )

    for ep, tp in others:
        greet(ep, tp)

    loads = [
        pltpu.make_async_copy(src, dst, load_sem.at[i])
        for i, (src, dst) in enumerate(
            ((gate_hbm, gate_vmem), (up_hbm, up_vmem), (down_hbm, down_vmem))
        )
    ]
    weights = ((value_own, value_full), (gate_own, gate_full), (out_own, out_full))
    pl.semaphore_wait(barrier, len(others))

    def slot_rows(index):
        return pl.ds(pl.multiple_of(index * slots, slots), slots)

    own_rows = pltpu.make_async_copy(
        outgoing.at[slot_rows(q), :], rows_all.at[t, slot_rows(q), :], own_sem
    )
    own_rows.start()
    a_copies = []
    for i in range(1, groups_ep):
        there = lax.rem(q + i, groups_ep)
        copy = remote(
            outgoing.at[slot_rows(there), :],
            rows_all.at[t, slot_rows(q), :],
            send_a.at[i],
            recv_a.at[i],
            there,
            t,
        )
        copy.start()
        a_copies.append(copy)

    def sends(d, s):
        return (z >= s) & (z < chips - 1) if d == 0 else (z + s < chips) & (z > 0)

    def comes(d, s):
        return z >= 1 + s if d == 0 else z + 1 + s < chips

    def sent(d, s):
        return (z - s if d == 0 else z + s) * 2 + core

    def came(d, s):
        return sent(d, s + 1)

    def beside(d):
        return t + 2 if d == 0 else t - 2

    def quarter(k, index, cut=0):
        own = weights[k][0]
        part = own.shape[0] // groups_ep
        if cut == 0:
            return pl.ds(pl.multiple_of(index * part, part), part)
        half = part // 2
        return pl.ds(pl.multiple_of(index * part + (cut - 1) * half, half), half)

    def first_leg(k, d, s):
        own, full = weights[k]
        place = columns(full, sent(d, s), own.shape[1], quarter(k, q))
        src = own.at[quarter(k, q), :] if s == 0 else place
        return remote(src, place, send_w1.at[k, d, s], recv_w1.at[k, d, s], q, beside(d))

    flip_low = q + 1 - 2 * lax.rem(q, 2)
    flip_high = q + 2 - 4 * lax.rem(q // 2, 2)
    square = groups_ep == 4

    def second_leg(k, d, s, j):
        own, full = weights[k]
        piece, there, cut = q, lax.rem(q + j, groups_ep), 0
        if square:
            piece = (flip_high, q, q, flip_low)[j]
            there = (flip_low, flip_low, flip_high, flip_high)[j]
            cut = (2, 0, 0, 1)[j]
        place = columns(full, came(d, s), own.shape[1], quarter(k, piece, cut))
        return remote(
            place, place, send_w2.at[k, d, s, j], recv_w2.at[k, d, s, j], there, t
        )

    direct = (1, 2) if square else tuple(range(1, groups_ep))
    relayed = (0, 3) if square else ()

    def own_leg(k):
        own, full = weights[k]
        place = columns(full, t, own.shape[1], pl.ds(0, own.shape[0]))
        last = chips - 1
        return remote(own, place, send_wp.at[k, 0, last], recv_wp.at[k, 0, last], q, partner)

    def pair_leg(k, d, s):
        own, full = weights[k]
        place = columns(full, came(d, s), own.shape[1], pl.ds(0, own.shape[0]))
        return remote(place, place, send_wp.at[k, d, s], recv_wp.at[k, d, s], q, partner)

    def pass_on(k, s):
        for d in range(2):
            pl.when(sends(d, s))(lambda d=d: first_leg(k, d, s).start())

    def take(k, s):
        for d in range(2):

            @pl.when(comes(d, s))
            def _(d=d):
                first_leg(k, d, s).wait_recv()
                for j in direct:
                    second_leg(k, d, s, j).start()

    def relay(k, s):
        for d in range(2):

            @pl.when(comes(d, s))
            def _(d=d):
                for j in direct:
                    second_leg(k, d, s, j).wait_recv()
                for j in relayed:
                    second_leg(k, d, s, j).start()

    def share(k, s):
        for d in range(2):

            @pl.when(comes(d, s))
            def _(d=d):
                for j in relayed:
                    second_leg(k, d, s, j).wait_recv()
                pair_leg(k, d, s).start()

    def row_leg(d, s):
        place = rows_all.at[sent(d, s)]
        return remote(place, place, send_r.at[d, s], recv_r.at[d, s], q, beside(d))

    def row_pair(d, s):
        place = rows_all.at[came(d, s)]
        return remote(place, place, send_rp.at[d, s], recv_rp.at[d, s], q, partner)

    def own_pair():
        place, last = rows_all.at[t], chips - 1
        return remote(place, place, send_rp.at[0, last], recv_rp.at[0, last], q, partner)

    def rows_on(s):
        for d in range(2):
            pl.when(sends(d, s))(lambda d=d: row_leg(d, s).start())

    def rows_in(s):
        for d in range(2):
            pl.when(comes(d, s))(lambda d=d: row_leg(d, s).wait_recv())

    def rows_share(s):
        for d in range(2):
            pl.when(comes(d, s))(lambda d=d: row_pair(d, s).start())

    steps = chips - 1
    for k in (0,):
        pass_on(k, 0)
    stored = [
        pltpu.make_async_copy(
            own, columns(full, t, own.shape[1], pl.ds(0, own.shape[0])), stage_sem.at[k]
        )
        for k, (own, full) in enumerate(weights)
    ]
    for copy in loads + stored:
        copy.start()
    if inside:
        rim = padded.shape[0] - mixer_in.shape[0]
        length = mixer_in.shape[0]
        normed[...] = rms_scale(mixer_in[...], pre_gain[...]).astype(jnp.bfloat16)

        @pl.when(me == 0)
        def _():
            padded[pl.ds(0, rim), :] = jnp.zeros((rim, padded.shape[1]), jnp.float32)

    def halo():
        return remote(
            padded.at[pl.ds(length, rim), :],
            padded.at[pl.ds(0, rim), :],
            send_h,
            recv_h,
            after // groups_tp,
            lax.rem(after, groups_tp),
        )

    def wait_weight(k):
        stored[k].wait()
        own_leg(k).wait_recv()
        for s in range(steps):
            for d in range(2):
                pl.when(comes(d, s))(lambda d=d, s=s: pair_leg(k, d, s).wait_recv())

    def glu_stage():
        wait_weight(0)
        wait_weight(1)
        wide = min(256, value_full.shape[1])

        @pl.loop(0, value_full.shape[1] // wide)
        def _(step):
            place = pl.ds(pl.multiple_of(step * wide, wide), wide)
            rows = normed[...]
            value = jnp.dot(rows, value_full[:, place], preferred_element_type=jnp.float32)
            gate = jnp.dot(rows, gate_full[:, place], preferred_element_type=jnp.float32)
            glu = (value * jax.nn.sigmoid(gate)).astype(jnp.bfloat16)
            padded[pl.ds(rim, length), place] = glu.astype(jnp.float32)

        pl.when(me < devices - 1)(lambda: halo().start())

    def conv_stage():
        pl.when(me > 0)(lambda: halo().wait_recv())
        taps = conv_kernel.shape[0]

        @pl.loop(0, conv.shape[1] // 128)
        def _(step):
            place = pl.ds(pl.multiple_of(step * 128, 128), 128)
            total = jnp.zeros((length, 128), jnp.float32)
            for tap in range(taps):
                rows = padded[pl.ds(rim - taps + 1 + tap, length), place]
                total = total + conv_kernel[pl.ds(tap, 1), place] * rows
            conv[:, place] = total

        some = min(64, length)

        @pl.loop(0, length // some)
        def _(step):
            place = pl.ds(pl.multiple_of(step * some, some), some)
            block = conv[place, :]
            centred = block - jnp.mean(block, axis=-1, keepdims=True)
            var = jnp.mean(centred * centred, axis=-1, keepdims=True)
            scaled = centred * lax.rsqrt(var + LAYER_EPSILON) * chan_gain[...]
            act[place, :] = (scaled * jax.nn.sigmoid(scaled)).astype(jnp.bfloat16)

    def out_stage():
        wait_weight(2)
        wide = min(256, out_full.shape[1])

        @pl.loop(0, out_full.shape[1] // wide)
        def _(step):
            place = pl.ds(pl.multiple_of(step * wide, wide), wide)
            projected[:, place] = jnp.dot(
                act[...], out_full[:, place], preferred_element_type=jnp.float32
            )

        some = min(64, length)

        @pl.loop(0, length // some)
        def _(step):
            place = pl.ds(pl.multiple_of(step * some, some), some)
            mixed[place, :] = rms_scale(projected[place, :], mix_gain[...]).astype(jnp.bfloat16)

    own_rows.wait()
    for copy in a_copies:
        copy.wait_recv()
    rows_on(0)
    pass_on(1, 0)
    pass_on(2, 0)
    own_pair().start()
    for k in range(3):
        own_leg(k).start()

    take(0, 0)
    for s in range(steps):
        rows_in(s)
        if s + 1 < steps:
            rows_on(s + 1)
        rows_share(s)
        if s == min(1, steps - 1):
            take(1, 0)
            take(2, 0)
            if steps > 1:
                for k in range(3):
                    pass_on(k, 1)
            for k in range(3):
                relay(k, 0)
    own_pair().wait_recv()
    for s in range(steps):
        for d in range(2):
            pl.when(comes(d, s))(lambda d=d: row_pair(d, s).wait_recv())
    for copy in loads:
        copy.wait()

    total = groups_tp * chunk
    tile = min(256, units)
    tiles = units // tile

    @pl.loop(0, local_experts * tiles)
    def _(step):
        expert, unit = step // tiles, step % tiles
        place = pl.ds(pl.multiple_of(unit * tile, tile), tile)
        rows = rows_all[...].reshape(total, width)
        gate = jnp.dot(rows, gate_vmem[expert, :, place], preferred_element_type=jnp.float32)
        up = jnp.dot(rows, up_vmem[expert, :, place], preferred_element_type=jnp.float32)
        gate = jnp.minimum(gate, CLAMP_LIMIT)
        up = jnp.clip(up, -CLAMP_LIMIT, CLAMP_LIMIT)
        act = (up + 1.0) * gate * jax.nn.sigmoid(SWISH_ALPHA * gate)
        slot = lax.rem(lax.broadcasted_iota(jnp.int32, act.shape, 0), slots)
        mine = (slot >= expert * capacity) & (slot < (expert + 1) * capacity)
        hidden[:, pl.ds(pl.multiple_of(step * tile, tile), tile)] = jnp.where(
            mine, act, 0.0
        ).astype(jnp.bfloat16)

    for k in range(3):
        if steps > 1:
            take(k, 1)
        if steps > 2:
            pass_on(k, 2)
    for k in range(3):
        share(k, 0)

    down_tile = min(256, width)

    @pl.loop(0, width // down_tile)
    def _(step):
        place = pl.ds(pl.multiple_of(step * down_tile, down_tile), down_tile)
        weight = down_vmem[:, :, place].reshape(local_experts * units, down_tile)
        part = jnp.dot(hidden[...], weight, preferred_element_type=jnp.float32)
        partial[:, :, place] = part.astype(jnp.bfloat16).reshape(groups_tp, chunk, down_tile)

    def sum_pair(owner):
        return remote(
            partial.at[owner * 2 + 1 - core],
            pair_in.at[owner],
            send_p.at[owner],
            recv_p.at[owner],
            q,
            partner,
        )

    def sum_leg(d, owner):
        return remote(
            partial.at[owner * 2 + core],
            ring_in.at[d, owner],
            send_z.at[d, owner],
            recv_z.at[d, owner],
            q,
            beside(d),
        )

    def behind(d):
        return z > 0 if d == 0 else z < chips - 1

    def add_pair(owner):
        sum_pair(owner).wait_recv()
        place = partial.at[owner * 2 + core]
        both = place[...].astype(jnp.float32) + pair_in[owner].astype(jnp.float32)
        place[...] = both.astype(jnp.bfloat16)

    def add_line(d, owner):
        sum_leg(d, owner).wait_recv()
        place = partial.at[owner * 2 + core]
        both = place[...].astype(jnp.float32) + ring_in[d, owner].astype(jnp.float32)
        place[...] = both.astype(jnp.bfloat16)

    def send_sums(step):
        for d in range(2):
            far = z if d == 0 else chips - 1 - z
            owner = z + chips - 1 - step if d == 0 else z + step - chips + 1

            @pl.when(far <= step)
            def _(d=d, owner=owner):
                add_pair(owner)
                pl.when(behind(d))(lambda: add_line(d, owner))
                sum_leg(d, owner).start()

    order = []
    for j in range(chips):
        order += [o for o in (chips - 1 - j, j) if o not in order]
    for owner in order:
        sum_pair(owner).start()
    for s in range(2, steps):
        for k in range(3):
            take(k, s)
            if s + 1 < steps:
                pass_on(k, s + 1)
    send_sums(0)
    for k in range(3):
        if steps > 1:
            relay(k, 1)
    if steps > 1:
        send_sums(1)
    for k in range(3):
        if steps > 1:
            share(k, 1)
        for s in range(2, steps):
            relay(k, s)
    for s in range(2, steps):
        for k in range(3):
            share(k, s)
    if inside:
        glu_stage()
    for step in range(2, steps):
        send_sums(step)
    if inside:
        conv_stage()
    add_pair(z)
    if inside:
        out_stage()
    for d in range(2):
        pl.when(behind(d))(lambda d=d: add_line(d, z))
    summed = partial[t].astype(jnp.float32)
    back_out[...] = summed.astype(jnp.bfloat16)

    def back_leg(i):
        there = lax.rem(q + i, groups_ep)
        return remote(
            back_out.at[slot_rows(there), :],
            back_in.at[slot_rows(q), :],
            send_b.at[i],
            recv_b.at[i],
            there,
            t,
        )

    for i in range(1, groups_ep):
        back_leg(i).start()
    back_in[slot_rows(q), :] = back_out[slot_rows(q), :]
    for i in range(1, groups_ep):
        back_leg(i).wait_recv()
    returned[...] = back_in[...]

    for k in range(3):
        own_leg(k).wait_send()
        if not inside:
            wait_weight(k)
    if inside:
        pl.when(me < devices - 1)(lambda: halo().wait_send())
    own_pair().wait_send()
    for s in range(steps):
        for d in range(2):

            @pl.when(sends(d, s))
            def _(d=d, s=s):
                row_leg(d, s).wait_send()
                for k in range(3):
                    first_leg(k, d, s).wait_send()

            @pl.when(comes(d, s))
            def _(d=d, s=s):
                row_pair(d, s).wait_send()
                for k in range(3):
                    for j in direct + relayed:
                        second_leg(k, d, s, j).wait_send()
                    pair_leg(k, d, s).wait_send()
    for owner in range(chips):
        sum_pair(owner).wait_send()
        pl.when(z < owner)(lambda owner=owner: sum_leg(0, owner).wait_send())
        pl.when(z > owner)(lambda owner=owner: sum_leg(1, owner).wait_send())
    for i in range(1, groups_ep):
        a_copies[i - 1].wait_send()
        back_leg(i).wait_send()


def exchange(
    mixer_in,
    pre_gain,
    conv_kernel,
    chan_gain,
    mix_gain,
    outgoing,
    glu_value,
    glu_gate,
    out_weight,
    gate_proj,
    up_proj,
    down_proj,
    capacity,
):
    groups_ep, groups_tp = lax.axis_size("ep"), lax.axis_size("tp")
    chips = groups_tp // 2
    chunk, width = outgoing.shape
    units = gate_proj.shape[2] * gate_proj.shape[0]
    half = jnp.bfloat16

    def gathered(shard):
        rows, cols = shard.shape
        if cols % 128:
            return jax.ShapeDtypeStruct((groups_tp, rows, cols), half)
        return jax.ShapeDtypeStruct((rows, groups_tp * cols), half)

    own = (glu_value, glu_gate, out_weight)
    dma = pltpu.SemaphoreType.DMA
    inside = glu_value.shape[1] % 128 == 0 and out_weight.shape[1] % 128 == 0
    full_shapes = [gathered(shard) for shard in own]
    back_shape = jax.ShapeDtypeStruct((chunk, width), half)
    length, channels = mixer_in.shape[0], conv_kernel.shape[1]
    rim = -(-(conv_kernel.shape[0] - 1) // 8) * 8
    anywhere, vmem = pl.BlockSpec(memory_space=pl.ANY), pl.BlockSpec(memory_space=pltpu.VMEM)
    own_scratch = []
    if inside:
        own_scratch = [pltpu.VMEM(shape.shape, half) for shape in full_shapes] + [
            pltpu.VMEM(mixer_in.shape, half),
            pltpu.VMEM((rim + length, channels), jnp.float32),
            pltpu.VMEM((length, channels), jnp.float32),
            pltpu.VMEM((length, channels), half),
            pltpu.VMEM(mixer_in.shape, jnp.float32),
        ]
        mixer_specs = [vmem] * 5
    else:
        mixer_specs = [anywhere] * 5
    outs = pl.pallas_call(
        functools.partial(exchange_kernel, groups_ep, groups_tp, capacity, inside),
        out_shape=[jax.ShapeDtypeStruct(mixer_in.shape, half), back_shape]
        if inside
        else full_shapes + [back_shape],
        in_specs=[vmem] + mixer_specs + [anywhere] * 6,
        out_specs=[vmem] * 2 if inside else [anywhere] * 3 + [vmem],
        scratch_shapes=own_scratch
        + [
            pltpu.VMEM((groups_tp, chunk, width), half),
            pltpu.VMEM((groups_tp * chunk, units), half),
            pltpu.VMEM((groups_tp, chunk, width), half),
            pltpu.VMEM((chips, chunk, width), half),
            pltpu.VMEM((2, chips, chunk, width), half),
            pltpu.VMEM((chunk, width), half),
            pltpu.VMEM((chunk, width), half),
            pltpu.VMEM(gate_proj.shape, half),
            pltpu.VMEM(up_proj.shape, half),
            pltpu.VMEM(down_proj.shape, half),
            dma((3,)),
            dma((3,)),
            dma,
            dma,
            dma,
            dma((groups_ep,)),
            dma((groups_ep,)),
            dma((2, chips)),
            dma((2, chips)),
            dma((2, chips)),
            dma((2, chips)),
            dma((3, 2, chips)),
            dma((3, 2, chips)),
            dma((3, 2, chips, groups_ep)),
            dma((3, 2, chips, groups_ep)),
            dma((3, 2, chips)),
            dma((3, 2, chips)),
            dma((chips,)),
            dma((chips,)),
            dma((2, chips)),
            dma((2, chips)),
            dma((groups_ep,)),
            dma((groups_ep,)),
        ],
        compiler_params=pltpu.CompilerParams(
            collective_id=0, has_side_effects=True, vmem_limit_bytes=60 * 1024 * 1024
        ),
    )(
        outgoing,
        mixer_in,
        pre_gain[None],
        conv_kernel,
        chan_gain[None],
        mix_gain[None],
        *own,
        gate_proj,
        up_proj,
        down_proj,
    )
    if inside:
        return None, outs[0], outs[1]
    full = [
        value if value.ndim == 2 else value.transpose(1, 0, 2).reshape(value.shape[1], -1)
        for value in outs[:3]
    ]
    return full, None, outs[3]


def mixer(full, mixer_in, pre_gain, conv_kernel, chan_gain, mix_gain):
    value_full, gate_full, out_full = full
    normed_mix = rms_scale(mixer_in, pre_gain).astype(jnp.bfloat16)
    value_pre = jnp.dot(normed_mix, value_full, preferred_element_type=jnp.float32)
    gate_mix = jnp.dot(normed_mix, gate_full, preferred_element_type=jnp.float32)
    gated_rows = (value_pre * jax.nn.sigmoid(gate_mix)).astype(jnp.bfloat16)
    kernel_width = conv_kernel.shape[0]
    length = gated_rows.shape[0]
    rim_rows = passed_along(gated_rows[length - (kernel_width - 1) :], ("ep", "tp"), 1)
    padded = jnp.concatenate([rim_rows, gated_rows], axis=0).astype(jnp.float32)
    conv_sum = jnp.zeros((length, gated_rows.shape[1]), jnp.float32)
    for offset in range(kernel_width):
        conv_sum = conv_sum + conv_kernel[offset] * padded[offset : offset + length]
    row_mean = jnp.mean(conv_sum, axis=-1, keepdims=True)
    centred = conv_sum - row_mean
    row_var = jnp.mean(centred * centred, axis=-1, keepdims=True)
    activated = jax.nn.silu(centred * lax.rsqrt(row_var + LAYER_EPSILON) * chan_gain).astype(
        jnp.bfloat16
    )
    projected = jnp.dot(activated, out_full, preferred_element_type=jnp.float32)
    mixed = rms_scale(projected, mix_gain).astype(jnp.bfloat16)
    return mixed


def on_device(
    mixer_in,
    pre_gain,
    glu_value,
    glu_gate,
    conv_kernel,
    chan_gain,
    out_weight,
    mix_gain,
    expert_in,
    ffn_gain,
    routing,
    route_weight,
    gate_proj,
    up_proj,
    down_proj,
    expert_gain,
):
    groups_ep = lax.axis_size("ep")
    local_experts = gate_proj.shape[0]
    experts = local_experts * groups_ep
    token_rows, top_count = routing.shape
    capacity = max(2, 3 * token_rows * top_count // (2 * experts))
    flat_route = routing.reshape(-1)
    onehot = (flat_route[:, None] == jnp.arange(experts, dtype=jnp.int32)[None, :]).astype(
        jnp.int32
    )
    before = jnp.cumsum(onehot, axis=0) - onehot
    rank_within = jnp.sum(before * onehot, axis=1)
    slots = -(-local_experts * capacity // 8) * 8
    slot_index = (
        flat_route // local_experts * slots + flat_route % local_experts * capacity + rank_within
    ).reshape(token_rows, top_count)
    slot_ids = jnp.arange(groups_ep * slots, dtype=jnp.int32)
    chosen = slot_index[None, :, :] == slot_ids[:, None, None]
    pick_matrix = jnp.sum(chosen.astype(jnp.float32), axis=2).astype(jnp.bfloat16)
    normed_exp = rms_scale(expert_in, ffn_gain).astype(jnp.bfloat16)
    outgoing = jnp.dot(pick_matrix, normed_exp, preferred_element_type=jnp.float32).astype(
        jnp.bfloat16
    )
    full, mixed, returned = exchange(
        mixer_in,
        pre_gain,
        conv_kernel,
        chan_gain,
        mix_gain,
        outgoing,
        glu_value,
        glu_gate,
        out_weight,
        gate_proj,
        up_proj,
        down_proj,
        capacity,
    )
    if mixed is None:
        mixed = mixer(full, mixer_in, pre_gain, conv_kernel, chan_gain, mix_gain)
    combined = jnp.zeros((token_rows, returned.shape[1]), jnp.float32)
    for column in range(top_count):
        combined = combined + route_weight[:, column][:, None] * returned[
            slot_index[:, column]
        ].astype(jnp.float32)
    routed = rms_scale(combined, expert_gain).astype(jnp.bfloat16)
    return (mixed, routed)


def solution(mesh):
    in_specs = (
        P(("ep", "tp"), None),
        P(),
        P(None, "tp"),
        P(None, "tp"),
        P(),
        P(),
        P(None, "tp"),
        P(),
        P(("ep", "tp"), None),
        P(),
        P(("ep", "tp"), None),
        P(("ep", "tp"), None),
        P("ep", None, "tp"),
        P("ep", None, "tp"),
        P("ep", "tp", None),
        P(),
    )
    out_specs = (P(("ep", "tp"), None), P(("ep", "tp"), None))
    return jax.shard_map(
        on_device, mesh=mesh, in_specs=in_specs, out_specs=out_specs, check_vma=False
    )
```

profile of v0, /device:TPU:0, one launch (start us, length us, event | category | flops | bytes accessed | tf_op | source)
XLA Modules:
  0.0 122.0 jit_solution(7959748216942881703)
XLA Ops:
  0.6 0.8 copy.28
  1.4 0.1 eq.30
  1.5 0.1 fusion.6
  1.6 0.1 reduce_window_sum.11
  1.7 0.2 select_reduce_fusion
  1.9 0.1 reduce_sum.39
  2.0 0.2 fusion.11
  2.2 0.1 copy.33
  2.3 0.1 convert_reduce_fusion
  2.4 1.0 fusion
  3.4 2.0 %convolution_convert_fusion.outgoing = bf16[96,2048]{1,0:T(8,128)(2,1)} fusion(bf16[32,2048]{1,0:T(8,128)(2,1)} %param.24, f32[2048]{0:T(1024)} %param.25, f32[32]{0:T(128)S(1)} %add_rsqrt_fusion.1, bf16[96,32]{0,1:T(8,128)(2,1)S(1)} %convert_reduce_fusion), kind=kOutput, calls=%fused_computation.2 | convolution fusion | flops 13041664 | bytes 538752 | tf_op jit(solution)/shard_map/dot_general | solution.py:748
  5.4 0.0 copy-start.1
  5.4 0.0 copy-start
  5.4 109.6 %shard_map.167 = (bf16[256,2048]{1,0:T(8,128)(2,1)}, bf16[96,2048]{1,0:T(8,128)(2,1)}) custom-call(bf16[96,2048]{1,0:T(8,128)(2,1)} %convolution_convert_fusion.outgoing, bf16[256,2048]{1,0:T(8,128)(2,1)} %mixer_in.1, f32[1,2048]{1,0:T(1,128)} %bitcast.8, f32[31,1024]{1,0:T(8,128)} %conv_kernel.1, f32[1,1024]{1,0:T(1,128)} %bitcast.10, f32[1,2048]{1,0:T(1,128)} %bitcast.9, ...), custom_call_target="tpu_custom_call" | custom-call | tf_op jit(solution)/shard_map/pallas_call | solution.py:620
  115.0 1.8 %gather_fusion = bf16[32,2048]{1,0:T(8,128)(2,1)S(1)} fusion(bf16[96,2048]{1,0:T(8,128)(2,1)} %get-tuple-element.5, s32[1024]{0:T(1024)S(1)} %get-tuple-element.11), kind=kCustom, calls=%fused_computation | custom fusion | bytes 262272 | tf_op jit(solution)/shard_map/gather | solution.py:770
  116.8 1.8 %gather_fusion.1 = bf16[32,2048]{1,0:T(8,128)(2,1)S(1)} fusion(bf16[96,2048]{1,0:T(8,128)(2,1)} %get-tuple-element.5, s32[1024]{0:T(1024)S(1)} %get-tuple-element.10), kind=kCustom, calls=%fused_computation.1 | custom fusion | bytes 262272 | tf_op jit(solution)/shard_map/gather | solution.py:770
  118.6 0.0 copy-done.1
  118.6 0.2 multiply_reduce_fusion
  118.9 0.0 copy-done
  118.9 0.8 multiply_convert_fusion
  119.7 2.3 %copy.35 = bf16[256,2048]{1,0:T(8,128)(2,1)} copy(bf16[256,2048]{1,0:T(8,128)(2,1)} %get-tuple-element.14) | data formatting | bytes 2097152
  (5 shorter events, 0.1 us)
Async XLA Ops:
  5.4 113.2 %copy-start.1 = (f32[32,2]{0,1:T(2,128)S(1)}, f32[32,2]{0,1:T(2,128)}, u32[]{:S(2)}) copy-start(f32[32,2]{0,1:T(2,128)} %param.27) | copy-start | bytes 772
  5.4 113.5 %copy-start = (f32[2048]{0:T(1024)S(1)}, f32[2048]{0:T(1024)}, u32[]{:S(2)}) copy-start(f32[2048]{0:T(1024)} %param.31) | copy-start | bytes 24580
where the time goes:
time: 122 us
  Pallas kernels  110 us (90%)
  local copies, waits for them, and re-layouts  6.99 us (6%)
  other arithmetic  2.72 us (2%)
  matrix products  1.97 us (2%)
    pallas_call x1, Pallas kernels, exchange(): pl.pallas_call(functools.partial(exchange_kernel, groups_ep, groups_tp, c...  110 us
    gather x2, local copies, waits for them, and re-layouts, on_device(): returned[slot_index[:, column]].astype(jnp.float32)  3.63 us
    unnamed x6, local copies, waits for them, and re-layouts  3.07 us

commit v1 on v0

--- a/solution.py
+++ b/solution.py
@@ -684,6 +684,775 @@
     return full, None, outs[3]
 
 
+def flipped(index, bit):
+    return index + bit - 2 * bit * lax.rem(index // bit, 2)
+
+
+def across(index, distance):
+    bit = 1
+    while bit <= distance:
+        if distance & bit:
+            index = flipped(index, bit)
+        bit *= 2
+    return index
+
+
+def fused_kernel(
+    groups_ep,
+    groups_tp,
+    capacity,
+    expert_in,
+    ffn_gain,
+    routes,
+    shares,
+    expert_gain,
+    mixer_hbm,
+    pre_gain,
+    conv_kernel,
+    chan_gain,
+    mix_gain,
+    value_own,
+    gate_own,
+    out_own,
+    gate_hbm,
+    up_hbm,
+    down_hbm,
+    mixed,
+    routed,
+    value_full,
+    gate_full,
+    out_full,
+    mixer_in,
+    normed,
+    padded,
+    tail_out,
+    tail_in,
+    conv,
+    act,
+    projected,
+    info,
+    rows_all,
+    picked,
+    hidden,
+    partial,
+    pair_in,
+    ring_in,
+    back_in,
+    gate_vmem,
+    up_vmem,
+    down_vmem,
+    load_sem,
+    stage_sem,
+    send_h,
+    recv_h,
+    send_rz,
+    recv_rz,
+    send_rx,
+    recv_rx,
+    send_rd,
+    recv_rd,
+    send_rp,
+    recv_rp,
+    send_w1,
+    recv_w1,
+    send_w2,
+    recv_w2,
+    send_wp,
+    recv_wp,
+    send_p,
+    recv_p,
+    send_z,
+    recv_z,
+    send_b,
+    recv_b,
+):
+    q = lax.axis_index("ep")
+    t = lax.axis_index("tp")
+    chips = groups_tp // 2
+    z, core = t // 2, t % 2
+    partner = z * 2 + 1 - core
+    tokens, width = expert_in.shape
+    slots = partial.shape[2]
+    local_experts, _, units = gate_vmem.shape
+    top_count = routes.shape[0]
+    half_tokens = tokens // 2
+
+    def remote(src, dst, send, recv, ep, tp):
+        return pltpu.make_async_remote_copy(
+            src_ref=src,
+            dst_ref=dst,
+            send_sem=send,
+            recv_sem=recv,
+            device_id=(ep, tp),
+            device_id_type=pl.DeviceIdType.MESH,
+        )
+
+    barrier = pltpu.get_barrier_semaphore()
+    others = [(lax.rem(q + i, groups_ep), t) for i in range(1, groups_ep)]
+    others += [(q, lax.rem(z + i, chips) * 2 + core) for i in range(1, chips)]
+    others += [(q, partner)]
+    me, devices = q * groups_tp + t, groups_ep * groups_tp
+    after, ahead = lax.rem(me + 1, devices), lax.rem(me + devices - 1, devices)
+    others += [(n // groups_tp, lax.rem(n, groups_tp)) for n in (after, ahead)]
+    for ep, tp in others:
+        pl.semaphore_signal(
+            barrier, inc=1, device_id=(ep, tp), device_id_type=pl.DeviceIdType.MESH
+        )
+
+    weights = ((value_own, value_full), (gate_own, gate_full), (out_own, out_full))
+    stored = [
+        pltpu.make_async_copy(
+            own, columns(full, t, own.shape[1], pl.ds(0, own.shape[0])), stage_sem.at[k]
+        )
+        for k, (own, full) in enumerate(weights)
+    ]
+    mixer_load = pltpu.make_async_copy(mixer_hbm, mixer_in, load_sem.at[3])
+    loads = [
+        pltpu.make_async_copy(src, dst, load_sem.at[i])
+        for i, (src, dst) in enumerate(
+            ((gate_hbm, gate_vmem), (up_hbm, up_vmem), (down_hbm, down_vmem))
+        )
+    ]
+    mixer_load.start()
+    for copy in stored + loads:
+        copy.start()
+
+    rows_all[0, t, :, pl.ds(0, width)] = rms_scale(expert_in[...], ffn_gain[...]).astype(
+        jnp.bfloat16
+    )
+    lanes = 128
+    expert_ids = lax.broadcasted_iota(jnp.int32, (lanes, tokens), 0)
+    chosen = [routes[pl.ds(k, 1), :] == expert_ids for k in range(top_count)]
+    named = sum(c.astype(jnp.float32) for c in chosen)
+    earlier = lax.broadcasted_iota(jnp.int32, (tokens, tokens), 0) < lax.broadcasted_iota(
+        jnp.int32, (tokens, tokens), 1
+    )
+    rank = jnp.dot(
+        named.astype(jnp.bfloat16),
+        earlier.astype(jnp.float32).astype(jnp.bfloat16),
+        preferred_element_type=jnp.float32,
+    )
+    group_ids = expert_ids // local_experts
+    base = group_ids * slots + (expert_ids - group_ids * local_experts) * capacity
+    spot = rank + base.astype(jnp.float32)
+    facts = jnp.zeros((lanes, tokens), jnp.float32)
+    for k in range(top_count):
+        slot = jnp.sum(jnp.where(chosen[k], spot, 0.0), axis=0, keepdims=True)
+        facts = facts + jnp.where(expert_ids == k, slot, 0.0)
+        facts = facts + jnp.where(expert_ids == top_count + k, shares[pl.ds(k, 1), :], 0.0)
+    info[...] = facts.T
+    rows_all[0, t, :, pl.ds(width, lanes)] = info[...].astype(jnp.bfloat16)
+
+    pl.semaphore_wait(barrier, len(others))
+
+    def row_z(m):
+        place = rows_all.at[0, t]
+        return remote(place, place, send_rz.at[m], recv_rz.at[m], q, across(z, m) * 2 + core)
+
+    def row_beside(b, m):
+        owner = across(z, m) * 2 + core
+        return remote(
+            rows_all.at[0, owner],
+            rows_all.at[1 + b, owner],
+            send_rx.at[b, m],
+            recv_rx.at[b, m],
+            flipped(q, 1 + b),
+            t,
+        )
+
+    def row_far(b, m):
+        owner = across(z, m) * 2 + core
+        some = pl.ds(b * half_tokens, half_tokens)
+        return remote(
+            rows_all.at[2 - b, owner, some, :],
+            rows_all.at[3, owner, some, :],
+            send_rd.at[b, m],
+            recv_rd.at[b, m],
+            flipped(q, 1 + b),
+            t,
+        )
+
+    def row_pair(j, m):
+        place = rows_all.at[j, across(z, m) * 2 + core]
+        return remote(place, place, send_rp.at[j, m], recv_rp.at[j, m], q, partner)
+
+    def rows_here(m):
+        if m:
+            row_z(m).wait_recv()
+        for b in range(2):
+            row_beside(b, m).start()
+        row_pair(0, m).start()
+
+    def rows_beside(m):
+        for b in range(2):
+            row_beside(b, m).wait_recv()
+            row_far(1 - b, m).start()
+            row_pair(1 + b, m).start()
+
+    def rows_far(m):
+        for b in range(2):
+            row_far(b, m).wait_recv()
+        row_pair(3, m).start()
+
+    def sends(d, s):
+        return (z >= s) & (z < chips - 1) if d == 0 else (z + s < chips) & (z > 0)
+
+    def comes(d, s):
+        return z >= 1 + s if d == 0 else z + 1 + s < chips
+
+    def sent(d, s):
+        return (z - s if d == 0 else z + s) * 2 + core
+
+    def came(d, s):
+        return sent(d, s + 1)
+
+    def beside(d):
+        return t + 2 if d == 0 else t - 2
+
+    def quarter(k, index, cut=0):
+        own = weights[k][0]
+        part = own.shape[0] // groups_ep
+        if cut == 0:
+            return pl.ds(pl.multiple_of(index * part, part), part)
+        half = part // 2
+        return pl.ds(pl.multiple_of(index * part + (cut - 1) * half, half), half)
+
+    def first_leg(k, d, s):
+        own, full = weights[k]
+        place = columns(full, sent(d, s), own.shape[1], quarter(k, q))
+        src = own.at[quarter(k, q), :] if s == 0 else place
+        return remote(src, place, send_w1.at[k, d, s], recv_w1.at[k, d, s], q, beside(d))
+
+    flip_low, flip_high = flipped(q, 1), flipped(q, 2)
+    direct, relayed = (1, 2), (0, 3)
+
+    def second_leg(k, d, s, j):
+        own, full = weights[k]
+        piece = (flip_high, q, q, flip_low)[j]
+        there = (flip_low, flip_low, flip_high, flip_high)[j]
+        cut = (2, 0, 0, 1)[j]
+        place = columns(full, came(d, s), own.shape[1], quarter(k, piece, cut))
+        return remote(
+            place, place, send_w2.at[k, d, s, j], recv_w2.at[k, d, s, j], there, t
+        )
+
+    def own_leg(k):
+        own, full = weights[k]
+        place = columns(full, t, own.shape[1], pl.ds(0, own.shape[0]))
+        last = chips - 1
+        return remote(own, place, send_wp.at[k, 0, last], recv_wp.at[k, 0, last], q, partner)
+
+    def pair_leg(k, d, s):
+        own, full = weights[k]
+        place = columns(full, came(d, s), own.shape[1], pl.ds(0, own.shape[0]))
+        return remote(place, place, send_wp.at[k, d, s], recv_wp.at[k, d, s], q, partner)
+
+    def pass_on(k, s):
+        if s < steps:
+            for d in range(2):
+                pl.when(sends(d, s))(lambda d=d: first_leg(k, d, s).start())
+
+    def take(k, s):
+        if s < steps:
+            for d in range(2):
+
+                @pl.when(comes(d, s))
+                def _(d=d):
+                    first_leg(k, d, s).wait_recv()
+                    for j in direct:
+                        second_leg(k, d, s, j).start()
+
+            pass_on(k, s + 1)
+
+    def relay(k, s):
+        if s < steps:
+            for d in range(2):
+
+                @pl.when(comes(d, s))
+                def _(d=d):
+                    for j in direct:
+                        second_leg(k, d, s, j).wait_recv()
+                    for j in relayed:
+                        second_leg(k, d, s, j).start()
+
+    def share(k, s):
+        if s < steps:
+            for d in range(2):
+
+                @pl.when(comes(d, s))
+                def _(d=d):
+                    for j in relayed:
+                        second_leg(k, d, s, j).wait_recv()
+                    pair_leg(k, d, s).start()
+
+    def wait_plane(k, m):
+        if m == 0:
+            stored[k].wait()
+            own_leg(k).wait_recv()
+            return
+        plane = across(z, m)
+        d = (plane > z).astype(jnp.int32)
+        s = (plane - z) * (2 * d - 1) - 1
+        own, full = weights[k]
+        place = columns(
+            full, plane * 2 + 1 - core, own.shape[1], pl.ds(0, own.shape[0])
+        )
+        remote(
+            place, place, send_wp.at[k, d, s], recv_wp.at[k, d, s], q, partner
+        ).wait_recv()
+
+    length = mixer_in.shape[0]
+    rim = padded.shape[0] - length
+
+    def norm_stage():
+        mixer_load.wait()
+        some = min(64, length)
+
+        @pl.loop(0, length // some)
+        def _(step):
+            place = pl.ds(pl.multiple_of(step * some, some), some)
+            normed[place, :] = rms_scale(mixer_in[place, :], pre_gain[...]).astype(jnp.bfloat16)
+
+    def glu_stage(m):
+        wait_plane(0, m)
+        wait_plane(1, m)
+        wide = 2 * value_own.shape[1]
+        place = pl.ds(pl.multiple_of(across(z, m) * wide, wide), wide)
+        rows = normed[...]
+        value = jnp.dot(rows, value_full[:, place], preferred_element_type=jnp.float32)
+        gate = jnp.dot(rows, gate_full[:, place], preferred_element_type=jnp.float32)
+        glu = (value * jax.nn.sigmoid(gate)).astype(jnp.bfloat16)
+        padded[pl.ds(rim, length), place] = glu.astype(jnp.float32)
+        tail_out[:, place] = glu[length - rim :, :]
+
+    def halo():
+        return remote(
+            tail_out, tail_in, send_h, recv_h, after // groups_tp, lax.rem(after, groups_tp)
+        )
+
+    def conv_stage():
+        @pl.when(me > 0)
+        def _():
+            halo().wait_recv()
+            padded[pl.ds(0, rim), :] = tail_in[...].astype(jnp.float32)
+
+        @pl.when(me == 0)
+        def _():
+            padded[pl.ds(0, rim), :] = jnp.zeros((rim, padded.shape[1]), jnp.float32)
+
+        taps = conv_kernel.shape[0]
+
+        @pl.loop(0, conv.shape[1] // 128)
+        def _(step):
+            place = pl.ds(pl.multiple_of(step * 128, 128), 128)
+            total = jnp.zeros((length, 128), jnp.float32)
+            for tap in range(taps):
+                rows = padded[pl.ds(rim - taps + 1 + tap, length), place]
+                total = total + conv_kernel[pl.ds(tap, 1), place] * rows
+            conv[:, place] = total
+
+        some = min(64, length)
+
+        @pl.loop(0, length // some)
+        def _(step):
+            place = pl.ds(pl.multiple_of(step * some, some), some)
+            block = conv[place, :]
+            centred = block - jnp.mean(block, axis=-1, keepdims=True)
+            var = jnp.mean(centred * centred, axis=-1, keepdims=True)
+            scaled = centred * lax.rsqrt(var + LAYER_EPSILON) * chan_gain[...]
+            act[place, :] = (scaled * jax.nn.sigmoid(scaled)).astype(jnp.bfloat16)
+
+    def out_stage(m):
+        wait_plane(2, m)
+        wide = out_own.shape[1]
+        start = across(z, m) * 2 * wide
+        for i in range(2):
+            place = pl.ds(pl.multiple_of(start + i * wide, wide), wide)
+            projected[:, place] = jnp.dot(
+                act[...], out_full[:, place], preferred_element_type=jnp.float32
+            )
+
+    def mixed_stage():
+        some = min(64, length)
+
+        @pl.loop(0, length // some)
+        def _(step):
+            place = pl.ds(pl.multiple_of(step * some, some), some)
+            mixed[place, :] = rms_scale(projected[place, :], mix_gain[...]).astype(jnp.bfloat16)
+
+    total = groups_tp * slots
+    tile = min(256, units)
+    tiles = units // tile
+    down_tile = min(256, width)
+
+    def expert_stage(j):
+        for m in range(chips):
+            row_pair(j, m).wait_recv()
+        if j == 0:
+            for copy in loads:
+                copy.wait()
+        every = groups_tp * tokens
+        block = rows_all[j].reshape(every, width + lanes)
+        facts = block[:, width:].astype(jnp.float32)
+        slot_ids = lax.broadcasted_iota(jnp.int32, (every, total), 1).astype(jnp.float32)
+        owner = lax.broadcasted_iota(jnp.int32, (every, 1), 0) // tokens
+        first = (owner * slots).astype(jnp.float32)
+        low = (q * slots).astype(jnp.float32)
+        pick = jnp.zeros((every, total), jnp.float32)
+        for k in range(top_count):
+            local = facts[:, k : k + 1] - low
+            mine = (local >= 0.0) & (local < float(slots))
+            target = jnp.where(mine, local + first, -1.0)
+            pick = pick + (target == slot_ids).astype(jnp.float32)
+        picked[...] = jnp.dot(
+            pick.T.astype(jnp.bfloat16), block[:, :width], preferred_element_type=jnp.float32
+        ).astype(jnp.bfloat16)
+
+        @pl.loop(0, local_experts * tiles)
+        def _(step):
+            expert, unit = step // tiles, step % tiles
+            place = pl.ds(pl.multiple_of(unit * tile, tile), tile)
+            rows = picked[...]
+            gate = jnp.dot(rows, gate_vmem[expert, :, place], preferred_element_type=jnp.float32)
+            up = jnp.dot(rows, up_vmem[expert, :, place], preferred_element_type=jnp.float32)
+            gate = jnp.minimum(gate, CLAMP_LIMIT)
+            up = jnp.clip(up, -CLAMP_LIMIT, CLAMP_LIMIT)
+            unit_act = (up + 1.0) * gate * jax.nn.sigmoid(SWISH_ALPHA * gate)
+            slot = lax.rem(lax.broadcasted_iota(jnp.int32, unit_act.shape, 0), slots)
+            mine = (slot >= expert * capacity) & (slot < (expert + 1) * capacity)
+            hidden[:, pl.ds(pl.multiple_of(step * tile, tile), tile)] = jnp.where(
+                mine, unit_act, 0.0
+            ).astype(jnp.bfloat16)
+
+        @pl.loop(0, width // down_tile)
+        def _(step):
+            place = pl.ds(pl.multiple_of(step * down_tile, down_tile), down_tile)
+            weight = down_vmem[:, :, place].reshape(local_experts * units, down_tile)
+            part = jnp.dot(hidden[...], weight, preferred_element_type=jnp.float32)
+            partial[j, :, :, place] = part.astype(jnp.bfloat16).reshape(
+                groups_tp, slots, down_tile
+            )
+
+        for owner in owners:
+            sum_pair(j, owner).start()
+
+    owners = []
+    for i in range(chips):
+        owners += [o for o in (chips - 1 - i, i) if o not in owners]
+
+    def sum_pair(j, owner):
+        return remote(
+            partial.at[j, owner * 2 + 1 - core],
+            pair_in.at[j, owner],
+            send_p.at[j, owner],
+            recv_p.at[j, owner],
+            q,
+            partner,
+        )
+
+    def sum_leg(j, d, owner):
+        return remote(
+            partial.at[j, owner * 2 + core],
+            ring_in.at[j, d, owner],
+            send_z.at[j, d, owner],
+            recv_z.at[j, d, owner],
+            q,
+            beside(d),
+        )
+
+    def behind(d):
+        return z > 0 if d == 0 else z < chips - 1
+
+    def add_to(j, owner, other):
+        place = partial.at[j, owner * 2 + core]
+        both = place[...].astype(jnp.float32) + other[...].astype(jnp.float32)
+        place[...] = both.astype(jnp.bfloat16)
+
+    def add_pair(j, owner):
+        sum_pair(j, owner).wait_recv()
+        add_to(j, owner, pair_in.at[j, owner])
+
+    def add_line(j, d, owner):
+        sum_leg(j, d, owner).wait_recv()
+        add_to(j, owner, ring_in.at[j, d, owner])
+
+    def send_sums(j, step):
+        for d in range(2):
+            far = z if d == 0 else chips - 1 - z
+            owner = z + chips - 1 - step if d == 0 else z + step - chips + 1
+
+            @pl.when(far <= step)
+            def _(d=d, owner=owner):
+                add_pair(j, owner)
+                pl.when(behind(d))(lambda: add_line(j, d, owner))
+                sum_leg(j, d, owner).start()
+
+    def back_leg(j):
+        return remote(
+            partial.at[j, t], back_in.at[j], send_b.at[j], recv_b.at[j], across(q, j), t
+        )
+
+    def own_sums(j):
+        add_pair(j, z)
+        for d in range(2):
+            pl.when(behind(d))(lambda d=d: add_line(j, d, z))
+        if j:
+            back_leg(j).start()
+
+    def routed_stage():
+        facts = info[...]
+        total_rows = jnp.zeros((tokens, width), jnp.float32)
+        slot_ids = lax.broadcasted_iota(jnp.int32, (tokens, slots), 1)
+        for j in range(groups_ep):
+            if j:
+                back_leg(j).wait_recv()
+            block = partial[0, t] if j == 0 else back_in[j]
+            low = across(q, j) * slots
+            shared = jnp.zeros((tokens, slots), jnp.float32)
+            for k in range(top_count):
+                here = facts[:, k : k + 1] == (slot_ids + low).astype(jnp.float32)
+                share_of = facts[:, top_count + k : top_count + k + 1]
+                shared = shared + jnp.where(here, share_of, 0.0)
+            high = shared.astype(jnp.bfloat16)
+            rest = (shared - high.astype(jnp.float32)).astype(jnp.bfloat16)
+            for term in (high, rest):
+                total_rows = total_rows + jnp.dot(
+                    term, block, preferred_element_type=jnp.float32
+                )
+        routed[...] = rms_scale(total_rows, expert_gain[...]).astype(jnp.bfloat16)
+
+    steps = chips - 1
+    both = (0, 1)
+    for m in range(1, chips):
+        row_z(m).start()
+    rows_here(0)
+    for k in both:
+        pass_on(k, 0)
+    for k in both:
+        own_leg(k).start()
+    norm_stage()
+    for m in range(1, chips):
+        rows_here(m)
+        rows_beside(m - 1)
+    glu_stage(0)
+    own_leg(2).start()
+    for k in both:
+        take(k, 0)
+    pass_on(2, 0)
+    expert_stage(0)
+    rows_beside(chips - 1)
+    for m in range(chips):
+        rows_far(m)
+    for k in both:
+        relay(k, 0)
+    expert_stage(1)
+    for k in both:
+        take(k, 1)
+    take(2, 0)
+    send_sums(0, 0)
+    expert_stage(2)
+    send_sums(0, 1)
+    send_sums(1, 0)
+    for k in both:
+        relay(k, 1)
+        share(k, 0)
+    relay(2, 0)
+    for s in range(2, steps):
+        for k in both:
+            take(k, s)
+    take(2, 1)
+    expert_stage(3)
+    for step in range(2, steps):
+        send_sums(0, step)
+    send_sums(1, 1)
+    send_sums(2, 0)
+    own_sums(0)
+    for k in both:
+        share(k, 1)
+    for s in range(2, steps):
+        for k in both:
+            relay(k, s)
+    glu_stage(1)
+    for step in range(2, steps):
+        send_sums(1, step)
+    send_sums(2, 1)
+    send_sums(3, 0)
+    for s in range(2, steps):
+        for k in both:
+            share(k, s)
+    relay(2, 1)
+    for s in range(2, steps):
+        take(2, s)
+    own_sums(1)
+    glu_stage(2)
+    for step in range(2, steps):
+        send_sums(2, step)
+    send_sums(3, 1)
+    own_sums(2)
+    for m in range(3, chips):
+        glu_stage(m)
+    pl.when(me < devices - 1)(lambda: halo().start())
+    for s in range(2, steps):
+        relay(2, s)
+    share(2, 0)
+    for step in range(2, steps):
+        send_sums(3, step)
+    share(2, 1)
+    own_sums(3)
+    conv_stage()
+    for s in range(2, steps):
+        share(2, s)
+    for m in range(chips):
+        out_stage(m)
+    mixed_stage()
+    routed_stage()
+
+    for m in range(chips):
+        if m:
+            row_z(m).wait_send()
+        for b in range(2):
+            row_beside(b, m).wait_send()
+            row_far(b, m).wait_send()
+        for j in range(groups_ep):
+            row_pair(j, m).wait_send()
+    for k in range(3):
+        own_leg(k).wait_send()
+    pl.when(me < devices - 1)(lambda: halo().wait_send())
+    for s in range(steps):
+        for d in range(2):
+
+            @pl.when(sends(d, s))
+            def _(d=d, s=s):
+                for k in range(3):
+                    first_leg(k, d, s).wait_send()
+
+            @pl.when(comes(d, s))
+            def _(d=d, s=s):
+                for k in range(3):
+                    for j in direct + relayed:
+                        second_leg(k, d, s, j).wait_send()
+                    pair_leg(k, d, s).wait_send()
+    for j in range(groups_ep):
+        for owner in range(chips):
+            sum_pair(j, owner).wait_send()
+            pl.when(z < owner)(lambda j=j, owner=owner: sum_leg(j, 0, owner).wait_send())
+            pl.when(z > owner)(lambda j=j, owner=owner: sum_leg(j, 1, owner).wait_send())
+        if j:
+            back_leg(j).wait_send()
+
+
+def fused(
+    mixer_in,
+    pre_gain,
+    glu_value,
+    glu_gate,
+    conv_kernel,
+    chan_gain,
+    out_weight,
+    mix_gain,
+    expert_in,
+    ffn_gain,
+    routing,
+    route_weight,
+    gate_proj,
+    up_proj,
+    down_proj,
+    expert_gain,
+    capacity,
+    slots,
+):
+    groups_ep, groups_tp = lax.axis_size("ep"), lax.axis_size("tp")
+    chips = groups_tp // 2
+    tokens, width = expert_in.shape
+    length, channels = mixer_in.shape[0], conv_kernel.shape[1]
+    units = gate_proj.shape[2] * gate_proj.shape[0]
+    half, full = jnp.bfloat16, jnp.float32
+    dma = pltpu.SemaphoreType.DMA
+    rim = -(-(conv_kernel.shape[0] - 1) // 8) * 8
+    anywhere, vmem = pl.BlockSpec(memory_space=pl.ANY), pl.BlockSpec(memory_space=pltpu.VMEM)
+
+    def gathered(shard):
+        return pltpu.VMEM((shard.shape[0], groups_tp * shard.shape[1]), half)
+
+    return pl.pallas_call(
+        functools.partial(fused_kernel, groups_ep, groups_tp, capacity),
+        out_shape=[
+            jax.ShapeDtypeStruct(mixer_in.shape, half),
+            jax.ShapeDtypeStruct(expert_in.shape, half),
+        ],
+        in_specs=[vmem] * 5 + [anywhere] + [vmem] * 4 + [anywhere] * 6,
+        out_specs=[vmem] * 2,
+        scratch_shapes=[
+            gathered(glu_value),
+            gathered(glu_gate),
+            gathered(out_weight),
+            pltpu.VMEM(mixer_in.shape, half),
+            pltpu.VMEM(mixer_in.shape, half),
+            pltpu.VMEM((rim + length, channels), full),
+            pltpu.VMEM((rim, channels), half),
+            pltpu.VMEM((rim, channels), half),
+            pltpu.VMEM((length, channels), full),
+            pltpu.VMEM((length, channels), half),
+            pltpu.VMEM(mixer_in.shape, full),
+            pltpu.VMEM((tokens, 128), full),
+            pltpu.VMEM((groups_ep, groups_tp, tokens, width + 128), half),
+            pltpu.VMEM((groups_tp * slots, width), half),
+            pltpu.VMEM((groups_tp * slots, units), half),
+            pltpu.VMEM((groups_ep, groups_tp, slots, width), half),
+            pltpu.VMEM((groups_ep, chips, slots, width), half),
+            pltpu.VMEM((groups_ep, 2, chips, slots, width), half),
+            pltpu.VMEM((groups_ep, slots, width), half),
+            pltpu.VMEM(gate_proj.shape, half),
+            pltpu.VMEM(up_proj.shape, half),
+            pltpu.VMEM(down_proj.shape, half),
+            dma((4,)),
+            dma((3,)),
+            dma,
+            dma,
+            dma((chips,)),
+            dma((chips,)),
+            dma((2, chips)),
+            dma((2, chips)),
+            dma((2, chips)),
+            dma((2, chips)),
+            dma((groups_ep, chips)),
+            dma((groups_ep, chips)),
+            dma((3, 2, chips)),
+            dma((3, 2, chips)),
+            dma((3, 2, chips, 4)),
+            dma((3, 2, chips, 4)),
+            dma((3, 2, chips)),
+            dma((3, 2, chips)),
+            dma((groups_ep, chips)),
+            dma((groups_ep, chips)),
+            dma((groups_ep, 2, chips)),
+            dma((groups_ep, 2, chips)),
+            dma((groups_ep,)),
+            dma((groups_ep,)),
+        ],
+        compiler_params=pltpu.CompilerParams(
+            collective_id=0, has_side_effects=True, vmem_limit_bytes=60 * 1024 * 1024
+        ),
+    )(
+        expert_in,
+        ffn_gain[None],
+        routing.T,
+        route_weight.T,
+        expert_gain[None],
+        mixer_in,
+        pre_gain[None],
+        conv_kernel,
+        chan_gain[None],
+        mix_gain[None],
+        glu_value,
+        glu_gate,
+        out_weight,
+        gate_proj,
+        up_proj,
+        down_proj,
+    )
+
+
 def mixer(full, mixer_in, pre_gain, conv_kernel, chan_gain, mix_gain):
     value_full, gate_full, out_full = full
     normed_mix = rms_scale(mixer_in, pre_gain).astype(jnp.bfloat16)
@@ -731,13 +1500,39 @@
     experts = local_experts * groups_ep
     token_rows, top_count = routing.shape
     capacity = max(2, 3 * token_rows * top_count // (2 * experts))
+    slots = -(-local_experts * capacity // 8) * 8
+    chips = lax.axis_size("tp") // 2
+    lined_up = all(w.shape[1] % 128 == 0 for w in (glu_value, glu_gate, out_weight))
+    two_way = groups_ep == 4 and chips > 1 and chips & (chips - 1) == 0
+    if lined_up and two_way and groups_ep * slots <= 256:
+        return tuple(
+            fused(
+                mixer_in,
+                pre_gain,
+                glu_value,
+                glu_gate,
+                conv_kernel,
+                chan_gain,
+                out_weight,
+                mix_gain,
+                expert_in,
+                ffn_gain,
+                routing,
+                route_weight,
+                gate_proj,
+                up_proj,
+                down_proj,
+                expert_gain,
+                capacity,
+                slots,
+            )
+        )
     flat_route = routing.reshape(-1)
     onehot = (flat_route[:, None] == jnp.arange(experts, dtype=jnp.int32)[None, :]).astype(
         jnp.int32
     )
     before = jnp.cumsum(onehot, axis=0) - onehot
     rank_within = jnp.sum(before * onehot, axis=1)
-    slots = -(-local_experts * capacity // 8) * 8
     slot_index = (
         flat_route // local_experts * slots + flat_route % local_experts * capacity + rank_within
     ).reshape(token_rows, top_count)

time: 122 us -> 105 us (0.86)
  Pallas kernels: 110 us -> 100 us
  local copies, waits for them, and re-layouts: 6.99 us -> 3.87 us
  other arithmetic: 2.72 us -> 0 us
  matrix products: 1.97 us -> 0 us
    pallas_call x1, Pallas kernels: 110 us -> 100 us  [fused(): pl.pallas_call(functools.partial(fused_kernel, groups_ep, groups_tp, capa...]
    gather x2 -> x0, local copies, waits for them, and re-layouts: 3.63 us -> none  [on_device(): returned[slot_index[:, column]].astype(jnp.float32)]
    dot_general x1 -> x0, matrix products: 1.97 us -> none  [on_device(): jnp.dot(pick_matrix, normed_exp, preferred_element_type=jnp.float32)]
    reduce_sum x4 -> x0, other arithmetic: 1.54 us -> none  [the longest x2 1.28 us: rms_scale(): jnp.mean(values * values, axis=-1, keepdims=True) + RMS_EPSILON]
    unnamed x6 -> x2, local copies, waits for them, and re-layouts: 3.07 us -> 3.87 us
where the time goes in v1:
time: 105 us
  Pallas kernels  100 us (95%)
  local copies, waits for them, and re-layouts  3.87 us (4%)
    pallas_call x1, Pallas kernels, fused(): pl.pallas_call(functools.partial(fused_kernel, groups_ep, groups_tp, capa...  100 us
    unnamed x2, local copies, waits for them, and re-layouts  3.87 us

profile of v1, /device:TPU:0, one launch (start us, length us, event | category | flops | bytes accessed | tf_op | source)
XLA Modules:
  0.0 104.6 jit_solution(17025467913312930734)
XLA Ops:
  0.6 100.1 %shard_map.167 = (bf16[256,2048]{1,0:T(8,128)(2,1)}, bf16[32,2048]{1,0:T(8,128)(2,1)}) custom-call(bf16[32,2048]{1,0:T(8,128)(2,1)} %expert_in.1, f32[1,2048]{1,0:T(1,128)} %bitcast.7, s32[2,32]{1,0:T(2,128)} %bitcast.12, f32[2,32]{1,0:T(2,128)} %bitcast.13, f32[1,2048]{1,0:T(1,128)} %bitcast.8, bf16[256,2048]{1,0:T(8,128)(2,1)} %mixer_hbm.1, ...), custom_call_target="tpu_custom_call" | custom-call | tf_op jit(solution)/shard_map/pallas_call | solution.py:1377
  100.7 2.3 %copy.20 = bf16[256,2048]{1,0:T(8,128)(2,1)} copy(bf16[256,2048]{1,0:T(8,128)(2,1)} %get-tuple-element.4) | data formatting | bytes 2097152
  103.0 1.6 %copy.21 = bf16[32,2048]{1,0:T(8,128)(2,1)} copy(bf16[32,2048]{1,0:T(8,128)(2,1)} %get-tuple-element.5) | data formatting | bytes 262144

commit v2 on v1

--- a/solution.py
+++ b/solution.py
@@ -701,16 +701,16 @@
     groups_ep,
     groups_tp,
     capacity,
-    expert_in,
-    ffn_gain,
-    routes,
-    shares,
-    expert_gain,
+    expert_in_hbm,
+    ffn_gain_hbm,
+    routes_hbm,
+    shares_hbm,
+    expert_gain_hbm,
     mixer_hbm,
-    pre_gain,
-    conv_kernel,
-    chan_gain,
-    mix_gain,
+    pre_gain_hbm,
+    conv_kernel_hbm,
+    chan_gain_hbm,
+    mix_gain_hbm,
     value_own,
     gate_own,
     out_own,
@@ -719,6 +719,15 @@
     down_hbm,
     mixed,
     routed,
+    expert_in,
+    ffn_gain,
+    routes,
+    shares,
+    expert_gain,
+    pre_gain,
+    conv_kernel,
+    chan_gain,
+    mix_gain,
     value_full,
     gate_full,
     out_full,
@@ -745,13 +754,10 @@
     stage_sem,
     send_h,
     recv_h,
-    send_rz,
+    send_rows,
     recv_rz,
-    send_rx,
     recv_rx,
-    send_rd,
     recv_rd,
-    send_rp,
     recv_rp,
     send_w1,
     recv_w1,
@@ -806,16 +812,43 @@
         )
         for k, (own, full) in enumerate(weights)
     ]
-    mixer_load = pltpu.make_async_copy(mixer_hbm, mixer_in, load_sem.at[3])
+    def loaded(number, src, dst):
+        return pltpu.make_async_copy(src, dst, load_sem.at[number])
+
+    row_loads = [
+        loaded(i, src, dst)
+        for i, (src, dst) in enumerate(
+            (
+                (expert_in_hbm, expert_in),
+                (ffn_gain_hbm, ffn_gain),
+                (routes_hbm, routes),
+                (shares_hbm, shares),
+            )
+        )
+    ]
+    mixer_loads = [
+        loaded(4 + i, src, dst)
+        for i, (src, dst) in enumerate(
+            (
+                (mixer_hbm, mixer_in),
+                (pre_gain_hbm, pre_gain),
+                (conv_kernel_hbm, conv_kernel),
+                (chan_gain_hbm, chan_gain),
+                (mix_gain_hbm, mix_gain),
+                (expert_gain_hbm, expert_gain),
+            )
+        )
+    ]
     loads = [
-        pltpu.make_async_copy(src, dst, load_sem.at[i])
+        loaded(10 + i, src, dst)
         for i, (src, dst) in enumerate(
             ((gate_hbm, gate_vmem), (up_hbm, up_vmem), (down_hbm, down_vmem))
         )
     ]
-    mixer_load.start()
-    for copy in stored + loads:
+    for copy in row_loads + mixer_loads + stored + loads:
         copy.start()
+    for copy in row_loads:
+        copy.wait()
 
     rows_all[0, t, :, pl.ds(0, width)] = rms_scale(expert_in[...], ffn_gain[...]).astype(
         jnp.bfloat16
@@ -845,17 +878,20 @@
 
     pl.semaphore_wait(barrier, len(others))
 
+    def took(ref, sem):
+        remote(ref, ref, sem, sem, q, partner).wait_send()
+
     def row_z(m):
         place = rows_all.at[0, t]
-        return remote(place, place, send_rz.at[m], recv_rz.at[m], q, across(z, m) * 2 + core)
+        return remote(place, place, send_rows.at[0], recv_rz.at[m], q, across(z, m) * 2 + core)
 
     def row_beside(b, m):
         owner = across(z, m) * 2 + core
         return remote(
             rows_all.at[0, owner],
             rows_all.at[1 + b, owner],
-            send_rx.at[b, m],
-            recv_rx.at[b, m],
+            send_rows.at[1],
+            recv_rx.at[m],
             flipped(q, 1 + b),
             t,
         )
@@ -866,33 +902,42 @@
         return remote(
             rows_all.at[2 - b, owner, some, :],
             rows_all.at[3, owner, some, :],
-            send_rd.at[b, m],
-            recv_rd.at[b, m],
+            send_rows.at[2],
+            recv_rd.at[m],
             flipped(q, 1 + b),
             t,
         )
 
     def row_pair(j, m):
         place = rows_all.at[j, across(z, m) * 2 + core]
-        return remote(place, place, send_rp.at[j, m], recv_rp.at[j, m], q, partner)
+        return remote(place, place, send_rows.at[3], recv_rp.at[j], q, partner)
+
+    def rows_start():
+        for m in range(1, chips):
+            row_z(m).start()
 
     def rows_here(m):
         if m:
-            row_z(m).wait_recv()
+            took(rows_all.at[0, t], recv_rz.at[m])
         for b in range(2):
             row_beside(b, m).start()
         row_pair(0, m).start()
 
     def rows_beside(m):
+        took(rows_all.at[0, pl.ds(0, 2)], recv_rx.at[m])
         for b in range(2):
-            row_beside(b, m).wait_recv()
             row_far(1 - b, m).start()
             row_pair(1 + b, m).start()
 
     def rows_far(m):
-        for b in range(2):
-            row_far(b, m).wait_recv()
+        took(rows_all.at[0, t], recv_rd.at[m])
         row_pair(3, m).start()
+
+    def rows_left():
+        took(rows_all.at[0, pl.ds(0, chips - 1)], send_rows.at[0])
+        took(rows_all.at[0, pl.ds(0, 2 * chips)], send_rows.at[1])
+        took(rows_all.at[0, pl.ds(0, chips)], send_rows.at[2])
+        took(rows_all.at[:, pl.ds(0, chips)], send_rows.at[3])
 
     def sends(d, s):
         return (z >= s) & (z < chips - 1) if d == 0 else (z + s < chips) & (z > 0)
@@ -917,95 +962,126 @@
         half = part // 2
         return pl.ds(pl.multiple_of(index * part + (cut - 1) * half, half), half)
 
-    def first_leg(k, d, s):
+    bundles = ((0, 1), (2,))
+
+    def first_leg(g, k, d, s):
         own, full = weights[k]
         place = columns(full, sent(d, s), own.shape[1], quarter(k, q))
         src = own.at[quarter(k, q), :] if s == 0 else place
-        return remote(src, place, send_w1.at[k, d, s], recv_w1.at[k, d, s], q, beside(d))
+        return remote(src, place, send_w1.at[d, s], recv_w1.at[g, d, s], q, beside(d))
 
     flip_low, flip_high = flipped(q, 1), flipped(q, 2)
     direct, relayed = (1, 2), (0, 3)
 
-    def second_leg(k, d, s, j):
+    def second_leg(g, k, d, s, j):
         own, full = weights[k]
         piece = (flip_high, q, q, flip_low)[j]
         there = (flip_low, flip_low, flip_high, flip_high)[j]
         cut = (2, 0, 0, 1)[j]
         place = columns(full, came(d, s), own.shape[1], quarter(k, piece, cut))
+        kind = 0 if j in direct else 1
         return remote(
-            place, place, send_w2.at[k, d, s, j], recv_w2.at[k, d, s, j], there, t
-        )
-
-    def own_leg(k):
+            place, place, send_w2.at[d, s], recv_w2.at[g, kind, d, s], there, t
+        )
+
+    def own_leg(g, k):
         own, full = weights[k]
         place = columns(full, t, own.shape[1], pl.ds(0, own.shape[0]))
         last = chips - 1
-        return remote(own, place, send_wp.at[k, 0, last], recv_wp.at[k, 0, last], q, partner)
-
-    def pair_leg(k, d, s):
+        return remote(own, place, send_wp.at[0, last], recv_wp.at[g, 0, last], q, partner)
+
+    def pair_leg(g, k, d, s):
         own, full = weights[k]
         place = columns(full, came(d, s), own.shape[1], pl.ds(0, own.shape[0]))
-        return remote(place, place, send_wp.at[k, d, s], recv_wp.at[k, d, s], q, partner)
-
-    def pass_on(k, s):
-        if s < steps:
-            for d in range(2):
-                pl.when(sends(d, s))(lambda d=d: first_leg(k, d, s).start())
-
-    def take(k, s):
-        if s < steps:
-            for d in range(2):
-
-                @pl.when(comes(d, s))
-                def _(d=d):
-                    first_leg(k, d, s).wait_recv()
-                    for j in direct:
-                        second_leg(k, d, s, j).start()
-
-            pass_on(k, s + 1)
-
-    def relay(k, s):
-        if s < steps:
-            for d in range(2):
-
-                @pl.when(comes(d, s))
-                def _(d=d):
-                    for j in direct:
-                        second_leg(k, d, s, j).wait_recv()
-                    for j in relayed:
-                        second_leg(k, d, s, j).start()
-
-    def share(k, s):
-        if s < steps:
-            for d in range(2):
-
-                @pl.when(comes(d, s))
-                def _(d=d):
-                    for j in relayed:
-                        second_leg(k, d, s, j).wait_recv()
-                    pair_leg(k, d, s).start()
-
-    def wait_plane(k, m):
+        return remote(place, place, send_wp.at[d, s], recv_wp.at[g, d, s], q, partner)
+
+    share_rows, share_wide = value_own.shape
+
+    def took_shares(quarters, sem):
+        tall = max(r for r in range(1, groups_ep + 1) if quarters % r == 0)
+        rows = pl.ds(0, share_rows // groups_ep * tall)
+        took(value_full.at[rows, pl.ds(0, quarters // tall * share_wide)], sem)
+
+    def passes(g, s):
+        for d in range(2):
+
+            @pl.when(sends(d, s))
+            def _(d=d):
+                for k in bundles[g]:
+                    first_leg(g, k, d, s).start()
+
+    def own_legs(g):
+        for k in bundles[g]:
+            own_leg(g, k).start()
+
+    def takes(g, s):
+        for d in range(2):
+
+            @pl.when(comes(d, s))
+            def _(d=d):
+                took_shares(len(bundles[g]), recv_w1.at[g, d, s])
+                if s + 1 < steps:
+
+                    @pl.when(sends(d, s + 1))
+                    def _():
+                        for k in bundles[g]:
+                            first_leg(g, k, d, s + 1).start()
+
+                for j in direct:
+                    for k in bundles[g]:
+                        second_leg(g, k, d, s, j).start()
+
+    def relays(g, s):
+        for d in range(2):
+
+            @pl.when(comes(d, s))
+            def _(d=d):
+                took_shares(2 * len(bundles[g]), recv_w2.at[g, 0, d, s])
+                for j in relayed:
+                    for k in bundles[g]:
+                        second_leg(g, k, d, s, j).start()
+
+    def shares_on(g, s):
+        for d in range(2):
+
+            @pl.when(comes(d, s))
+            def _(d=d):
+                took_shares(len(bundles[g]), recv_w2.at[g, 1, d, s])
+                for k in bundles[g]:
+                    pair_leg(g, k, d, s).start()
+
+    def wait_plane(g, m):
         if m == 0:
-            stored[k].wait()
-            own_leg(k).wait_recv()
+            for k in bundles[g]:
+                stored[k].wait()
+            took_shares(groups_ep * len(bundles[g]), recv_wp.at[g, 0, chips - 1])
             return
         plane = across(z, m)
         d = (plane > z).astype(jnp.int32)
         s = (plane - z) * (2 * d - 1) - 1
-        own, full = weights[k]
-        place = columns(
-            full, plane * 2 + 1 - core, own.shape[1], pl.ds(0, own.shape[0])
-        )
-        remote(
-            place, place, send_wp.at[k, d, s], recv_wp.at[k, d, s], q, partner
-        ).wait_recv()
+        took_shares(groups_ep * len(bundles[g]), recv_wp.at[g, d, s])
+
+    def shares_left():
+        took_shares(3 * groups_ep, send_wp.at[0, chips - 1])
+        for s in range(steps):
+            for d in range(2):
+
+                @pl.when(sends(d, s))
+                def _(d=d, s=s):
+                    took_shares(3, send_w1.at[d, s])
+
+                @pl.when(comes(d, s))
+                def _(d=d, s=s):
+                    took_shares(9, send_w2.at[d, s])
+                    took_shares(3 * groups_ep, send_wp.at[d, s])
 
     length = mixer_in.shape[0]
-    rim = padded.shape[0] - length
+    rim = padded.shape[1] - length
+    lane_blocks = padded.shape[0]
 
     def norm_stage():
-        mixer_load.wait()
+        for copy in mixer_loads:
+            copy.wait()
         some = min(64, length)
 
         @pl.loop(0, length // some)
@@ -1015,14 +1091,16 @@
 
     def glu_stage(m):
         wait_plane(0, m)
-        wait_plane(1, m)
         wide = 2 * value_own.shape[1]
         place = pl.ds(pl.multiple_of(across(z, m) * wide, wide), wide)
         rows = normed[...]
         value = jnp.dot(rows, value_full[:, place], preferred_element_type=jnp.float32)
         gate = jnp.dot(rows, gate_full[:, place], preferred_element_type=jnp.float32)
         glu = (value * jax.nn.sigmoid(gate)).astype(jnp.bfloat16)
-        padded[pl.ds(rim, length), place] = glu.astype(jnp.float32)
+        for i in range(wide // lanes):
+            padded[across(z, m) * (wide // lanes) + i, pl.ds(rim, length), :] = glu[
+                :, i * lanes : (i + 1) * lanes
+            ].astype(jnp.float32)
         tail_out[:, place] = glu[length - rim :, :]
 
     def halo():
@@ -1030,27 +1108,36 @@
             tail_out, tail_in, send_h, recv_h, after // groups_tp, lax.rem(after, groups_tp)
         )
 
-    def conv_stage():
+    def halo_start():
+        pl.when(me < devices - 1)(lambda: halo().start())
+
+    def conv_start():
         @pl.when(me > 0)
         def _():
             halo().wait_recv()
-            padded[pl.ds(0, rim), :] = tail_in[...].astype(jnp.float32)
+            for i in range(lane_blocks):
+                padded[i, pl.ds(0, rim), :] = tail_in[:, i * lanes : (i + 1) * lanes].astype(
+                    jnp.float32
+                )
 
         @pl.when(me == 0)
         def _():
-            padded[pl.ds(0, rim), :] = jnp.zeros((rim, padded.shape[1]), jnp.float32)
-
+            padded[:, pl.ds(0, rim), :] = jnp.zeros((lane_blocks, rim, lanes), jnp.float32)
+
+    def conv_stage(part):
         taps = conv_kernel.shape[0]
-
-        @pl.loop(0, conv.shape[1] // 128)
+        here = lane_blocks // chips
+
+        @pl.loop(part * here, (part + 1) * here)
         def _(step):
-            place = pl.ds(pl.multiple_of(step * 128, 128), 128)
-            total = jnp.zeros((length, 128), jnp.float32)
+            place = pl.ds(pl.multiple_of(step * lanes, lanes), lanes)
+            total = jnp.zeros((length, lanes), jnp.float32)
             for tap in range(taps):
-                rows = padded[pl.ds(rim - taps + 1 + tap, length), place]
+                rows = padded[step, pl.ds(rim - taps + 1 + tap, length), :]
                 total = total + conv_kernel[pl.ds(tap, 1), place] * rows
             conv[:, place] = total
 
+    def act_stage():
         some = min(64, length)
 
         @pl.loop(0, length // some)
@@ -1063,7 +1150,7 @@
             act[place, :] = (scaled * jax.nn.sigmoid(scaled)).astype(jnp.bfloat16)
 
     def out_stage(m):
-        wait_plane(2, m)
+        wait_plane(1, m)
         wide = out_own.shape[1]
         start = across(z, m) * 2 * wide
         for i in range(2):
@@ -1081,13 +1168,12 @@
             mixed[place, :] = rms_scale(projected[place, :], mix_gain[...]).astype(jnp.bfloat16)
 
     total = groups_tp * slots
-    tile = min(256, units)
+    tile = min(512, units)
     tiles = units // tile
-    down_tile = min(256, width)
-
-    def expert_stage(j):
-        for m in range(chips):
-            row_pair(j, m).wait_recv()
+    down_tile = min(512, width)
+
+    def pick_stage(j):
+        took(rows_all.at[0, pl.ds(0, chips)], recv_rp.at[j])
         if j == 0:
             for copy in loads:
                 copy.wait()
@@ -1108,9 +1194,10 @@
             pick.T.astype(jnp.bfloat16), block[:, :width], preferred_element_type=jnp.float32
         ).astype(jnp.bfloat16)
 
-        @pl.loop(0, local_experts * tiles)
-        def _(step):
-            expert, unit = step // tiles, step % tiles
+    def up_stage(j, expert):
+        @pl.loop(0, tiles)
+        def _(unit):
+            step = expert * tiles + unit
             place = pl.ds(pl.multiple_of(unit * tile, tile), tile)
             rows = picked[...]
             gate = jnp.dot(rows, gate_vmem[expert, :, place], preferred_element_type=jnp.float32)
@@ -1124,6 +1211,7 @@
                 mine, unit_act, 0.0
             ).astype(jnp.bfloat16)
 
+    def down_stage(j):
         @pl.loop(0, width // down_tile)
         def _(step):
             place = pl.ds(pl.multiple_of(step * down_tile, down_tile), down_tile)
@@ -1144,18 +1232,22 @@
         return remote(
             partial.at[j, owner * 2 + 1 - core],
             pair_in.at[j, owner],
-            send_p.at[j, owner],
-            recv_p.at[j, owner],
+            send_p.at[j],
+            recv_p.at[j],
             q,
             partner,
         )
 
-    def sum_leg(j, d, owner):
+    def owner_of(d, step):
+        return z + chips - 1 - step if d == 0 else z + step - chips + 1
+
+    def sum_leg(j, d, step):
+        owner = owner_of(d, step)
         return remote(
             partial.at[j, owner * 2 + core],
             ring_in.at[j, d, owner],
-            send_z.at[j, d, owner],
-            recv_z.at[j, d, owner],
+            send_z.at[d, step],
+            recv_z.at[j, d, step],
             q,
             beside(d),
         )
@@ -1168,45 +1260,54 @@
         both = place[...].astype(jnp.float32) + other[...].astype(jnp.float32)
         place[...] = both.astype(jnp.bfloat16)
 
-    def add_pair(j, owner):
-        sum_pair(j, owner).wait_recv()
-        add_to(j, owner, pair_in.at[j, owner])
-
-    def add_line(j, d, owner):
-        sum_leg(j, d, owner).wait_recv()
+    def add_line(j, d, owner, step):
+        took(partial.at[j, t], recv_z.at[j, d, step])
         add_to(j, owner, ring_in.at[j, d, owner])
 
     def send_sums(j, step):
+        if step == 0:
+            took(pair_in.at[j], recv_p.at[j])
         for d in range(2):
             far = z if d == 0 else chips - 1 - z
-            owner = z + chips - 1 - step if d == 0 else z + step - chips + 1
 
             @pl.when(far <= step)
-            def _(d=d, owner=owner):
-                add_pair(j, owner)
-                pl.when(behind(d))(lambda: add_line(j, d, owner))
-                sum_leg(j, d, owner).start()
+            def _(d=d):
+                owner = owner_of(d, step)
+                add_to(j, owner, pair_in.at[j, owner])
+                if step:
+                    pl.when(behind(d))(lambda: add_line(j, d, owner, step - 1))
+                sum_leg(j, d, step).start()
 
     def back_leg(j):
         return remote(
-            partial.at[j, t], back_in.at[j], send_b.at[j], recv_b.at[j], across(q, j), t
+            partial.at[j, t], back_in.at[j - 1], send_b, recv_b, across(q, j), t
         )
 
     def own_sums(j):
-        add_pair(j, z)
+        add_to(j, z, pair_in.at[j, z])
         for d in range(2):
-            pl.when(behind(d))(lambda d=d: add_line(j, d, z))
+            pl.when(behind(d))(lambda d=d: add_line(j, d, z, chips - 2))
         if j:
             back_leg(j).start()
 
+    def sums_left():
+        for j in range(groups_ep):
+            took(pair_in.at[j], send_p.at[j])
+        for d in range(2):
+            far = z if d == 0 else chips - 1 - z
+            for step in range(steps):
+                pl.when(far <= step)(
+                    lambda d=d, step=step: took(partial.at[:, 0], send_z.at[d, step])
+                )
+        took(back_in, send_b)
+
     def routed_stage():
+        took(back_in, recv_b)
         facts = info[...]
         total_rows = jnp.zeros((tokens, width), jnp.float32)
         slot_ids = lax.broadcasted_iota(jnp.int32, (tokens, slots), 1)
         for j in range(groups_ep):
-            if j:
-                back_leg(j).wait_recv()
-            block = partial[0, t] if j == 0 else back_in[j]
+            block = partial[0, t] if j == 0 else back_in[j - 1]
             low = across(q, j) * slots
             shared = jnp.zeros((tokens, slots), jnp.float32)
             for k in range(top_count):
@@ -1222,123 +1323,96 @@
         routed[...] = rms_scale(total_rows, expert_gain[...]).astype(jnp.bfloat16)
 
     steps = chips - 1
-    both = (0, 1)
-    for m in range(1, chips):
-        row_z(m).start()
+    rows_start()
     rows_here(0)
-    for k in both:
-        pass_on(k, 0)
-    for k in both:
-        own_leg(k).start()
+    rows_beside(0)
+    rows_far(0)
+    rows_here(1)
+    rows_here(2)
+    rows_beside(1)
     norm_stage()
-    for m in range(1, chips):
-        rows_here(m)
-        rows_beside(m - 1)
+    passes(0, 0)
+    rows_beside(2)
+    rows_here(3)
+    own_legs(1)
+    pick_stage(0)
+    up_stage(0, 0)
+    up_stage(0, 1)
+    takes(0, 0)
+    rows_beside(3)
+    down_stage(0)
+    pick_stage(1)
+    up_stage(1, 0)
+    passes(1, 0)
+    send_sums(0, 0)
+    up_stage(1, 1)
+    down_stage(1)
+    pick_stage(2)
+    own_legs(0)
+    takes(0, 1)
+    send_sums(1, 0)
+    relays(0, 0)
+    up_stage(2, 0)
+    up_stage(2, 1)
+    takes(1, 0)
+    down_stage(2)
+    rows_far(1)
+    rows_far(2)
+    send_sums(2, 0)
+    rows_far(3)
+    pick_stage(3)
+    takes(0, 2)
+    send_sums(1, 1)
+    up_stage(3, 0)
+    up_stage(3, 1)
+    relays(0, 1)
+    send_sums(0, 1)
+    takes(1, 1)
+    send_sums(0, 2)
+    down_stage(3)
+    send_sums(3, 0)
+    send_sums(2, 1)
+    relays(0, 2)
+    takes(1, 2)
+    send_sums(3, 1)
+    shares_on(0, 0)
+    send_sums(1, 2)
     glu_stage(0)
-    own_leg(2).start()
-    for k in both:
-        take(k, 0)
-    pass_on(2, 0)
-    expert_stage(0)
-    rows_beside(chips - 1)
-    for m in range(chips):
-        rows_far(m)
-    for k in both:
-        relay(k, 0)
-    expert_stage(1)
-    for k in both:
-        take(k, 1)
-    take(2, 0)
-    send_sums(0, 0)
-    expert_stage(2)
-    send_sums(0, 1)
-    send_sums(1, 0)
-    for k in both:
-        relay(k, 1)
-        share(k, 0)
-    relay(2, 0)
-    for s in range(2, steps):
-        for k in both:
-            take(k, s)
-    take(2, 1)
-    expert_stage(3)
-    for step in range(2, steps):
-        send_sums(0, step)
-    send_sums(1, 1)
-    send_sums(2, 0)
+    glu_stage(1)
+    relays(1, 0)
+    send_sums(3, 2)
+    shares_on(0, 1)
+    send_sums(2, 2)
     own_sums(0)
-    for k in both:
-        share(k, 1)
-    for s in range(2, steps):
-        for k in both:
-            relay(k, s)
-    glu_stage(1)
-    for step in range(2, steps):
-        send_sums(1, step)
-    send_sums(2, 1)
-    send_sums(3, 0)
-    for s in range(2, steps):
-        for k in both:
-            share(k, s)
-    relay(2, 1)
-    for s in range(2, steps):
-        take(2, s)
+    relays(1, 1)
+    shares_on(0, 2)
+    relays(1, 2)
+    glu_stage(3)
+    glu_stage(2)
+    own_sums(3)
+    halo_start()
+    conv_start()
     own_sums(1)
-    glu_stage(2)
-    for step in range(2, steps):
-        send_sums(2, step)
-    send_sums(3, 1)
+    conv_stage(3)
+    shares_on(1, 0)
+    conv_stage(2)
+    conv_stage(0)
+    shares_on(1, 1)
     own_sums(2)
-    for m in range(3, chips):
-        glu_stage(m)
-    pl.when(me < devices - 1)(lambda: halo().start())
-    for s in range(2, steps):
-        relay(2, s)
-    share(2, 0)
-    for step in range(2, steps):
-        send_sums(3, step)
-    share(2, 1)
-    own_sums(3)
-    conv_stage()
-    for s in range(2, steps):
-        share(2, s)
-    for m in range(chips):
-        out_stage(m)
+    conv_stage(1)
+    shares_on(1, 2)
+    act_stage()
+    out_stage(1)
+    out_stage(0)
+    out_stage(2)
+    out_stage(3)
     mixed_stage()
     routed_stage()
 
-    for m in range(chips):
-        if m:
-            row_z(m).wait_send()
-        for b in range(2):
-            row_beside(b, m).wait_send()
-            row_far(b, m).wait_send()
-        for j in range(groups_ep):
-            row_pair(j, m).wait_send()
-    for k in range(3):
-        own_leg(k).wait_send()
+    rows_left()
+    shares_left()
     pl.when(me < devices - 1)(lambda: halo().wait_send())
-    for s in range(steps):
-        for d in range(2):
-
-            @pl.when(sends(d, s))
-            def _(d=d, s=s):
-                for k in range(3):
-                    first_leg(k, d, s).wait_send()
-
-            @pl.when(comes(d, s))
-            def _(d=d, s=s):
-                for k in range(3):
-                    for j in direct + relayed:
-                        second_leg(k, d, s, j).wait_send()
-                    pair_leg(k, d, s).wait_send()
-    for j in range(groups_ep):
-        for owner in range(chips):
-            sum_pair(j, owner).wait_send()
-            pl.when(z < owner)(lambda j=j, owner=owner: sum_leg(j, 0, owner).wait_send())
-            pl.when(z > owner)(lambda j=j, owner=owner: sum_leg(j, 1, owner).wait_send())
-        if j:
-            back_leg(j).wait_send()
+    sums_left()
 
 
 def fused(
@@ -1369,7 +1443,7 @@
     half, full = jnp.bfloat16, jnp.float32
     dma = pltpu.SemaphoreType.DMA
     rim = -(-(conv_kernel.shape[0] - 1) // 8) * 8
-    anywhere, vmem = pl.BlockSpec(memory_space=pl.ANY), pl.BlockSpec(memory_space=pltpu.VMEM)
+    vmem = pl.BlockSpec(memory_space=pltpu.VMEM)
 
     def gathered(shard):
         return pltpu.VMEM((shard.shape[0], groups_tp * shard.shape[1]), half)
@@ -1380,15 +1454,24 @@
             jax.ShapeDtypeStruct(mixer_in.shape, half),
             jax.ShapeDtypeStruct(expert_in.shape, half),
         ],
-        in_specs=[vmem] * 5 + [anywhere] + [vmem] * 4 + [anywhere] * 6,
+        in_specs=[pl.BlockSpec(memory_space=pltpu.HBM)] * 16,
         out_specs=[vmem] * 2,
         scratch_shapes=[
+            pltpu.VMEM(expert_in.shape, half),
+            pltpu.VMEM((1, width), full),
+            pltpu.VMEM(routing.shape[::-1], routing.dtype),
+            pltpu.VMEM(route_weight.shape[::-1], full),
+            pltpu.VMEM((1, width), full),
+            pltpu.VMEM((1, width), full),
+            pltpu.VMEM(conv_kernel.shape, full),
+            pltpu.VMEM((1, channels), full),
+            pltpu.VMEM((1, width), full),
             gathered(glu_value),
             gathered(glu_gate),
             gathered(out_weight),
             pltpu.VMEM(mixer_in.shape, half),
             pltpu.VMEM(mixer_in.shape, half),
-            pltpu.VMEM((rim + length, channels), full),
+            pltpu.VMEM((channels // 128, rim + length, 128), full),
             pltpu.VMEM((rim, channels), half),
             pltpu.VMEM((rim, channels), half),
             pltpu.VMEM((length, channels), full),
@@ -1401,34 +1484,31 @@
             pltpu.VMEM((groups_ep, groups_tp, slots, width), half),
             pltpu.VMEM((groups_ep, chips, slots, width), half),
             pltpu.VMEM((groups_ep, 2, chips, slots, width), half),
-            pltpu.VMEM((groups_ep, slots, width), half),
+            pltpu.VMEM((groups_ep - 1, slots, width), half),
             pltpu.VMEM(gate_proj.shape, half),
             pltpu.VMEM(up_proj.shape, half),
             pltpu.VMEM(down_proj.shape, half),
-            dma((4,)),
+            dma((13,)),
             dma((3,)),
             dma,
             dma,
+            dma((4,)),
             dma((chips,)),
             dma((chips,)),
+            dma((chips,)),
+            dma((groups_ep,)),
+            dma((2, chips - 1)),
+            dma((2, 2, chips - 1)),
+            dma((2, chips - 1)),
+            dma((2, 2, 2, chips - 1)),
             dma((2, chips)),
-            dma((2, chips)),
-            dma((2, chips)),
-            dma((2, chips)),
-            dma((groups_ep, chips)),
-            dma((groups_ep, chips)),
-            dma((3, 2, chips)),
-            dma((3, 2, chips)),
-            dma((3, 2, chips, 4)),
-            dma((3, 2, chips, 4)),
-            dma((3, 2, chips)),
-            dma((3, 2, chips)),
-            dma((groups_ep, chips)),
-            dma((groups_ep, chips)),
-            dma((groups_ep, 2, chips)),
-            dma((groups_ep, 2, chips)),
+            dma((2, 2, chips)),
             dma((groups_ep,)),
             dma((groups_ep,)),
+            dma((2, chips - 1)),
+            dma((groups_ep, 2, chips - 1)),
+            dma,
+            dma,
         ],
         compiler_params=pltpu.CompilerParams(
             collective_id=0, has_side_effects=True, vmem_limit_bytes=60 * 1024 * 1024

time: 105 us -> 83.5 us (0.80)
  Pallas kernels: 100 us -> 78.8 us
    pallas_call x1, Pallas kernels: 100 us -> 78.8 us  [fused(): pl.pallas_call(functools.partial(fused_kernel, groups_ep, groups_tp, capa...]
where the time goes in v2:
time: 83.5 us; the launch traced here: 83.3 us
  Pallas kernels  78.8 us (94%)
  local copies, waits for them, and re-layouts  3.87 us (5%)
    pallas_call x1, Pallas kernels, fused(): pl.pallas_call(functools.partial(fused_kernel, groups_ep, groups_tp, capa...  78.8 us
    unnamed x2, local copies, waits for them, and re-layouts  3.87 us

profile of v2, /device:TPU:0, one launch (start us, length us, event | category | flops | bytes accessed | tf_op | source)
XLA Modules:
  0.0 83.3 jit_solution(9783523072134079047)
XLA Ops:
  0.6 78.8 %shard_map.167 = (bf16[256,2048]{1,0:T(8,128)(2,1)}, bf16[32,2048]{1,0:T(8,128)(2,1)}) custom-call(bf16[32,2048]{1,0:T(8,128)(2,1)} %expert_in_hbm.1, f32[1,2048]{1,0:T(1,128)} %bitcast.7, s32[2,32]{1,0:T(2,128)} %bitcast.12, f32[2,32]{1,0:T(2,128)} %bitcast.13, f32[1,2048]{1,0:T(1,128)} %bitcast.8, bf16[256,2048]{1,0:T(8,128)(2,1)} %mixer_hbm.1, ...), custom_call_target="tpu_custom_call" | custom-call | tf_op jit(solution)/shard_map/pallas_call | solution.py:1451
  79.5 2.3 %copy.20 = bf16[256,2048]{1,0:T(8,128)(2,1)} copy(bf16[256,2048]{1,0:T(8,128)(2,1)} %get-tuple-element.4) | data formatting | bytes 2097152
  81.8 1.6 %copy.21 = bf16[32,2048]{1,0:T(8,128)(2,1)} copy(bf16[32,2048]{1,0:T(8,128)(2,1)} %get-tuple-element.5) | data formatting | bytes 262144

commit v3 on v2

--- a/solution.py
+++ b/solution.py
@@ -710,15 +710,14 @@
     pre_gain_hbm,
     conv_kernel_hbm,
     chan_gain_hbm,
-    mix_gain_hbm,
     value_own,
     gate_own,
     out_own,
     gate_hbm,
     up_hbm,
     down_hbm,
-    mixed,
-    routed,
+    projected_hbm,
+    routed_hbm,
     expert_in,
     ffn_gain,
     routes,
@@ -727,7 +726,6 @@
     pre_gain,
     conv_kernel,
     chan_gain,
-    mix_gain,
     value_full,
     gate_full,
     out_full,
@@ -739,6 +737,7 @@
     conv,
     act,
     projected,
+    routed,
     info,
     rows_all,
     picked,
@@ -752,6 +751,7 @@
     down_vmem,
     load_sem,
     stage_sem,
+    out_sem,
     send_h,
     recv_h,
     send_rows,
@@ -834,13 +834,12 @@
                 (pre_gain_hbm, pre_gain),
                 (conv_kernel_hbm, conv_kernel),
                 (chan_gain_hbm, chan_gain),
-                (mix_gain_hbm, mix_gain),
                 (expert_gain_hbm, expert_gain),
             )
         )
     ]
     loads = [
-        loaded(10 + i, src, dst)
+        loaded(9 + i, src, dst)
         for i, (src, dst) in enumerate(
             ((gate_hbm, gate_vmem), (up_hbm, up_vmem), (down_hbm, down_vmem))
         )
@@ -964,10 +963,19 @@
 
     bundles = ((0, 1), (2,))
 
+    side = lax.rem(lax.rem(q, 2) + q // 2, 2)
+
+    def piece_rows(g, k):
+        if g == 0:
+            return quarter(k, q)
+        half = weights[k][0].shape[0] // 2
+        return pl.ds(pl.multiple_of(side * half, half), half)
+
     def first_leg(g, k, d, s):
         own, full = weights[k]
-        place = columns(full, sent(d, s), own.shape[1], quarter(k, q))
-        src = own.at[quarter(k, q), :] if s == 0 else place
+        rows = piece_rows(g, k)
+        place = columns(full, sent(d, s), own.shape[1], rows)
+        src = own.at[rows, :] if s == 0 else place
         return remote(src, place, send_w1.at[d, s], recv_w1.at[g, d, s], q, beside(d))
 
     flip_low, flip_high = flipped(q, 1), flipped(q, 2)
@@ -978,6 +986,8 @@
         piece = (flip_high, q, q, flip_low)[j]
         there = (flip_low, flip_low, flip_high, flip_high)[j]
         cut = (2, 0, 0, 1)[j]
+        if g:
+            piece, cut = side * 2 + j - 1, 0
         place = columns(full, came(d, s), own.shape[1], quarter(k, piece, cut))
         kind = 0 if j in direct else 1
         return remote(
@@ -1019,7 +1029,7 @@
 
             @pl.when(comes(d, s))
             def _(d=d):
-                took_shares(len(bundles[g]), recv_w1.at[g, d, s])
+                took_shares(2, recv_w1.at[g, d, s])
                 if s + 1 < steps:
 
                     @pl.when(sends(d, s + 1))
@@ -1046,7 +1056,7 @@
 
             @pl.when(comes(d, s))
             def _(d=d):
-                took_shares(len(bundles[g]), recv_w2.at[g, 1, d, s])
+                took_shares(2, recv_w2.at[g, 1 - g, d, s])
                 for k in bundles[g]:
                     pair_leg(g, k, d, s).start()
 
@@ -1068,11 +1078,11 @@
 
                 @pl.when(sends(d, s))
                 def _(d=d, s=s):
-                    took_shares(3, send_w1.at[d, s])
+                    took_shares(4, send_w1.at[d, s])
 
                 @pl.when(comes(d, s))
                 def _(d=d, s=s):
-                    took_shares(9, send_w2.at[d, s])
+                    took_shares(8, send_w2.at[d, s])
                     took_shares(3 * groups_ep, send_wp.at[d, s])
 
     length = mixer_in.shape[0]
@@ -1158,14 +1168,14 @@
             projected[:, place] = jnp.dot(
                 act[...], out_full[:, place], preferred_element_type=jnp.float32
             )
-
-    def mixed_stage():
-        some = min(64, length)
-
-        @pl.loop(0, length // some)
-        def _(step):
-            place = pl.ds(pl.multiple_of(step * some, some), some)
-            mixed[place, :] = rms_scale(projected[place, :], mix_gain[...]).astype(jnp.bfloat16)
+        projected_out(m).start()
+
+    def projected_out(m):
+        both = 2 * out_own.shape[1]
+        place = pl.ds(pl.multiple_of(across(z, m) * both, both), both)
+        return pltpu.make_async_copy(
+            projected.at[:, place], projected_hbm.at[:, place], out_sem.at[m]
+        )
 
     total = groups_tp * slots
     tile = min(512, units)
@@ -1321,98 +1331,142 @@
                     term, block, preferred_element_type=jnp.float32
                 )
         routed[...] = rms_scale(total_rows, expert_gain[...]).astype(jnp.bfloat16)
+        routed_out().start()
+
+    def routed_out():
+        return pltpu.make_async_copy(routed, routed_hbm, out_sem.at[chips])
 
     steps = chips - 1
     rows_start()
     rows_here(0)
     rows_beside(0)
+    rows_here(1)
     rows_far(0)
-    rows_here(1)
+    passes(0, 0)
+    rows_beside(1)
     rows_here(2)
-    rows_beside(1)
+    passes(1, 0)
+    rows_here(3)
     norm_stage()
-    passes(0, 0)
+    pick_stage(0)
+    own_legs(1)
     rows_beside(2)
-    rows_here(3)
-    own_legs(1)
-    pick_stage(0)
     up_stage(0, 0)
     up_stage(0, 1)
+    rows_beside(3)
     takes(0, 0)
-    rows_beside(3)
     down_stage(0)
     pick_stage(1)
+    rows_far(1)
     up_stage(1, 0)
-    passes(1, 0)
     send_sums(0, 0)
+    rows_far(2)
     up_stage(1, 1)
     down_stage(1)
+    send_sums(0, 1)
+    takes(0, 1)
     pick_stage(2)
-    own_legs(0)
-    takes(0, 1)
     send_sums(1, 0)
-    relays(0, 0)
+    takes(1, 0)
     up_stage(2, 0)
     up_stage(2, 1)
-    takes(1, 0)
     down_stage(2)
-    rows_far(1)
-    rows_far(2)
     send_sums(2, 0)
     rows_far(3)
+    send_sums(0, 2)
+    send_sums(2, 1)
+    relays(0, 0)
     pick_stage(3)
-    takes(0, 2)
-    send_sums(1, 1)
     up_stage(3, 0)
     up_stage(3, 1)
+    down_stage(3)
+    send_sums(2, 2)
+    takes(0, 2)
+    send_sums(3, 0)
+    send_sums(1, 1)
+    send_sums(3, 1)
     relays(0, 1)
-    send_sums(0, 1)
+    own_legs(0)
+    relays(0, 2)
+    shares_on(1, 0)
     takes(1, 1)
-    send_sums(0, 2)
-    down_stage(3)
-    send_sums(3, 0)
-    send_sums(2, 1)
-    relays(0, 2)
-    takes(1, 2)
-    send_sums(3, 1)
     shares_on(0, 0)
     send_sums(1, 2)
     glu_stage(0)
+    own_sums(0)
+    shares_on(0, 1)
+    send_sums(3, 2)
     glu_stage(1)
-    relays(1, 0)
-    send_sums(3, 2)
-    shares_on(0, 1)
-    send_sums(2, 2)
-    own_sums(0)
-    relays(1, 1)
     shares_on(0, 2)
-    relays(1, 2)
+    takes(1, 2)
     glu_stage(3)
+    own_sums(2)
     glu_stage(2)
+    halo_start()
+    shares_on(1, 1)
+    own_sums(1)
     own_sums(3)
-    halo_start()
     conv_start()
-    own_sums(1)
+    conv_stage(2)
+    shares_on(1, 2)
+    conv_stage(0)
     conv_stage(3)
-    shares_on(1, 0)
-    conv_stage(2)
-    conv_stage(0)
-    shares_on(1, 1)
-    own_sums(2)
     conv_stage(1)
-    shares_on(1, 2)
     act_stage()
     out_stage(1)
-    out_stage(0)
     out_stage(2)
     out_stage(3)
-    mixed_stage()
+    out_stage(0)
     routed_stage()
 
     rows_left()
     shares_left()
     pl.when(me < devices - 1)(lambda: halo().wait_send())
     sums_left()
+    for m in range(chips):
+        projected_out(m).wait()
+    routed_out().wait()
+
+
+def finish_kernel(
+    projected_hbm,
+    routed_hbm,
+    gain_hbm,
+    mixed_hbm,
+    routed_out_hbm,
+    projected,
+    routed,
+    gain,
+    mixed,
+    in_sem,
+    out_sem,
+):
+    length = projected.shape[0]
+    parts = mixed_hbm.shape[0] // min(64, mixed_hbm.shape[0])
+    some = length // parts
+
+    def row_copy(i, src, dst, sem):
+        rows = pl.ds(i * some, some)
+        return pltpu.make_async_copy(src.at[rows, :], dst.at[rows, :], sem.at[i])
+
+    gain_in = pltpu.make_async_copy(gain_hbm, gain, in_sem.at[parts])
+    routed_in = pltpu.make_async_copy(routed_hbm, routed, in_sem.at[parts + 1])
+    routed_back = pltpu.make_async_copy(routed, routed_out_hbm, out_sem.at[parts])
+    gain_in.start()
+    for i in range(parts):
+        row_copy(i, projected_hbm, projected, in_sem).start()
+    routed_in.start()
+    gain_in.wait()
+    for i in range(parts):
+        row_copy(i, projected_hbm, projected, in_sem).wait()
+        rows = pl.ds(i * some, some)
+        mixed[rows, :] = rms_scale(projected[rows, :], gain[...]).astype(jnp.bfloat16)
+        row_copy(i, mixed, mixed_hbm, out_sem).start()
+    routed_in.wait()
+    routed_back.start()
+    for i in range(parts):
+        row_copy(i, mixed, mixed_hbm, out_sem).wait()
+    routed_back.wait()
 
 
 def fused(
@@ -1443,19 +1497,19 @@
     half, full = jnp.bfloat16, jnp.float32
     dma = pltpu.SemaphoreType.DMA
     rim = -(-(conv_kernel.shape[0] - 1) // 8) * 8
-    vmem = pl.BlockSpec(memory_space=pltpu.VMEM)
+    anywhere = pl.BlockSpec(memory_space=pl.ANY)
 
     def gathered(shard):
         return pltpu.VMEM((shard.shape[0], groups_tp * shard.shape[1]), half)
 
-    return pl.pallas_call(
+    projected, routed = pl.pallas_call(
         functools.partial(fused_kernel, groups_ep, groups_tp, capacity),
         out_shape=[
-            jax.ShapeDtypeStruct(mixer_in.shape, half),
+            jax.ShapeDtypeStruct(mixer_in.shape, full),
             jax.ShapeDtypeStruct(expert_in.shape, half),
         ],
-        in_specs=[pl.BlockSpec(memory_space=pltpu.HBM)] * 16,
-        out_specs=[vmem] * 2,
+        in_specs=[anywhere] * 15,
+        out_specs=[anywhere] * 2,
         scratch_shapes=[
             pltpu.VMEM(expert_in.shape, half),
             pltpu.VMEM((1, width), full),
@@ -1465,7 +1519,6 @@
             pltpu.VMEM((1, width), full),
             pltpu.VMEM(conv_kernel.shape, full),
             pltpu.VMEM((1, channels), full),
-            pltpu.VMEM((1, width), full),
             gathered(glu_value),
             gathered(glu_gate),
             gathered(out_weight),
@@ -1477,6 +1530,7 @@
             pltpu.VMEM((length, channels), full),
             pltpu.VMEM((length, channels), half),
             pltpu.VMEM(mixer_in.shape, full),
+            pltpu.VMEM(expert_in.shape, half),
             pltpu.VMEM((tokens, 128), full),
             pltpu.VMEM((groups_ep, groups_tp, tokens, width + 128), half),
             pltpu.VMEM((groups_tp * slots, width), half),
@@ -1488,8 +1542,9 @@
             pltpu.VMEM(gate_proj.shape, half),
             pltpu.VMEM(up_proj.shape, half),
             pltpu.VMEM(down_proj.shape, half),
-            dma((13,)),
+            dma((12,)),
             dma((3,)),
+            dma((chips + 1,)),
             dma,
             dma,
             dma((4,)),
@@ -1523,7 +1578,6 @@
         pre_gain[None],
         conv_kernel,
         chan_gain[None],
-        mix_gain[None],
         glu_value,
         glu_gate,
         out_weight,
@@ -1531,6 +1585,25 @@
         up_proj,
         down_proj,
     )
+    parts = length // min(64, length)
+    return pl.pallas_call(
+        finish_kernel,
+        out_shape=[
+            jax.ShapeDtypeStruct(mixer_in.shape, half),
+            jax.ShapeDtypeStruct(expert_in.shape, half),
+        ],
+        in_specs=[anywhere] * 3,
+        out_specs=[anywhere] * 2,
+        scratch_shapes=[
+            pltpu.VMEM(mixer_in.shape, full),
+            pltpu.VMEM(expert_in.shape, half),
+            pltpu.VMEM((1, width), full),
+            pltpu.VMEM(mixer_in.shape, half),
+            dma((parts + 2,)),
+            dma((parts + 1,)),
+        ],
+        compiler_params=pltpu.CompilerParams(vmem_limit_bytes=60 * 1024 * 1024),
+    )(projected, routed, mix_gain[None])
 
 
 def mixer(full, mixer_in, pre_gain, conv_kernel, chan_gain, mix_gain):

time: 83.5 us -> 77.6 us (0.929)
  the two profiles are of different devices: /device:TPU:0 before, /device:TPU:4 now
where the time goes in v3:
time: 77.6 us; the launch traced here: 77.3 us
  Pallas kernels  76.5 us (99%)
  between operations  0.8 us (1%)
    pallas_call x1, Pallas kernels, fused(): pl.pallas_call(functools.partial(fused_kernel, groups_ep, groups_tp, capa...  74 us
    pallas_call x1, Pallas kernels, fused(): pl.pallas_call(finish_kernel, out_shape=[jax.ShapeDtypeStruct(mixer_in.sh...  2.53 us

profile of v3, /device:TPU:4, one launch (start us, length us, event | category | flops | bytes accessed | tf_op | source)
XLA Modules:
  0.0 77.3 jit_solution(18228455299722421114)
XLA Ops:
  0.6 74.0 %shard_map.167 = (f32[256,2048]{1,0:T(8,128)}, bf16[32,2048]{1,0:T(8,128)(2,1)}) custom-call(bf16[32,2048]{1,0:T(8,128)(2,1)} %expert_in_hbm.1, f32[1,2048]{1,0:T(1,128)} %bitcast.7, s32[2,32]{1,0:T(2,128)} %bitcast.12, f32[2,32]{1,0:T(2,128)} %bitcast.13, f32[1,2048]{1,0:T(1,128)} %bitcast.8, bf16[256,2048]{1,0:T(8,128)(2,1)} %mixer_hbm.1, ...), custom_call_target="tpu_custom_call" | custom-call | tf_op jit(solution)/shard_map/pallas_call | solution.py:1505
  74.7 2.5 %shard_map.168 = (bf16[256,2048]{1,0:T(8,128)(2,1)}, bf16[32,2048]{1,0:T(8,128)(2,1)}) custom-call(f32[256,2048]{1,0:T(8,128)} %get-tuple-element.4.projected_hbm, bf16[32,2048]{1,0:T(8,128)(2,1)} %get-tuple-element.5.routed_hbm, f32[1,2048]{1,0:T(1,128)} %bitcast.10), custom_call_target="tpu_custom_call" | custom-call | tf_op jit(solution)/shard_map/pallas_call | solution.py:1589

commit v4 on v3

--- a/solution.py
+++ b/solution.py
@@ -991,19 +991,19 @@
         place = columns(full, came(d, s), own.shape[1], quarter(k, piece, cut))
         kind = 0 if j in direct else 1
         return remote(
-            place, place, send_w2.at[d, s], recv_w2.at[g, kind, d, s], there, t
+            place, place, send_w2, recv_w2.at[g, kind, d, s], there, t
         )
 
     def own_leg(g, k):
         own, full = weights[k]
         place = columns(full, t, own.shape[1], pl.ds(0, own.shape[0]))
         last = chips - 1
-        return remote(own, place, send_wp.at[0, last], recv_wp.at[g, 0, last], q, partner)
+        return remote(own, place, send_wp.at[k], recv_wp.at[g, 0, last], q, partner)
 
     def pair_leg(g, k, d, s):
         own, full = weights[k]
         place = columns(full, came(d, s), own.shape[1], pl.ds(0, own.shape[0]))
-        return remote(place, place, send_wp.at[d, s], recv_wp.at[g, d, s], q, partner)
+        return remote(place, place, send_wp.at[k], recv_wp.at[g, d, s], q, partner)
 
     share_rows, share_wide = value_own.shape
 
@@ -1072,18 +1072,15 @@
         took_shares(groups_ep * len(bundles[g]), recv_wp.at[g, d, s])
 
     def shares_left():
-        took_shares(3 * groups_ep, send_wp.at[0, chips - 1])
+        took_shares(8 * steps, send_w2)
+        for k in range(3):
+            took_shares(groups_ep * chips, send_wp.at[k])
         for s in range(steps):
             for d in range(2):
 
                 @pl.when(sends(d, s))
                 def _(d=d, s=s):
                     took_shares(4, send_w1.at[d, s])
-
-                @pl.when(comes(d, s))
-                def _(d=d, s=s):
-                    took_shares(8, send_w2.at[d, s])
-                    took_shares(3 * groups_ep, send_wp.at[d, s])
 
     length = mixer_in.shape[0]
     rim = padded.shape[1] - length
@@ -1112,19 +1109,41 @@
                 :, i * lanes : (i + 1) * lanes
             ].astype(jnp.float32)
         tail_out[:, place] = glu[length - rim :, :]
-
-    def halo():
+        pl.when(me < devices - 1)(lambda: halo(place).start())
+
+    def halo(place):
         return remote(
-            tail_out, tail_in, send_h, recv_h, after // groups_tp, lax.rem(after, groups_tp)
-        )
-
-    def halo_start():
-        pl.when(me < devices - 1)(lambda: halo().start())
-
-    def conv_start():
+            tail_out.at[:, place],
+            tail_in.at[:, place],
+            send_h,
+            recv_h,
+            after // groups_tp,
+            lax.rem(after, groups_tp),
+        )
+
+    taps = conv_kernel.shape[0]
+    some = min(64, length)
+    head_steps = -(-rim // some)
+
+    def conv_rows(step, start, count):
+        place = pl.ds(pl.multiple_of(step * lanes, lanes), lanes)
+        total = jnp.zeros((count, lanes), jnp.float32)
+        for tap in range(taps):
+            rows = padded[step, pl.ds(rim + start - taps + 1 + tap, count), :]
+            total = total + conv_kernel[pl.ds(tap, 1), place] * rows
+        conv[pl.ds(start, count), place] = total
+
+    def conv_stage(part):
+        here = lane_blocks // chips
+
+        @pl.loop(part * here, (part + 1) * here)
+        def _(step):
+            conv_rows(step, rim, length - rim)
+
+    def conv_head():
         @pl.when(me > 0)
         def _():
-            halo().wait_recv()
+            took(tail_in, recv_h)
             for i in range(lane_blocks):
                 padded[i, pl.ds(0, rim), :] = tail_in[:, i * lanes : (i + 1) * lanes].astype(
                     jnp.float32
@@ -1134,23 +1153,12 @@
         def _():
             padded[:, pl.ds(0, rim), :] = jnp.zeros((lane_blocks, rim, lanes), jnp.float32)
 
-    def conv_stage(part):
-        taps = conv_kernel.shape[0]
-        here = lane_blocks // chips
-
-        @pl.loop(part * here, (part + 1) * here)
+        @pl.loop(0, lane_blocks)
         def _(step):
-            place = pl.ds(pl.multiple_of(step * lanes, lanes), lanes)
-            total = jnp.zeros((length, lanes), jnp.float32)
-            for tap in range(taps):
-                rows = padded[step, pl.ds(rim - taps + 1 + tap, length), :]
-                total = total + conv_kernel[pl.ds(tap, 1), place] * rows
-            conv[:, place] = total
-
-    def act_stage():
-        some = min(64, length)
-
-        @pl.loop(0, length // some)
+            conv_rows(step, 0, rim)
+
+    def act_rows(first, last):
+        @pl.loop(first, last)
         def _(step):
             place = pl.ds(pl.multiple_of(step * some, some), some)
             block = conv[place, :]
@@ -1158,6 +1166,12 @@
             var = jnp.mean(centred * centred, axis=-1, keepdims=True)
             scaled = centred * lax.rsqrt(var + LAYER_EPSILON) * chan_gain[...]
             act[place, :] = (scaled * jax.nn.sigmoid(scaled)).astype(jnp.bfloat16)
+
+    def act_tail():
+        act_rows(head_steps, length // some)
+
+    def act_head():
+        act_rows(0, head_steps)
 
     def out_stage(m):
         wait_plane(1, m)
@@ -1242,7 +1256,7 @@
         return remote(
             partial.at[j, owner * 2 + 1 - core],
             pair_in.at[j, owner],
-            send_p.at[j],
+            send_p,
             recv_p.at[j],
             q,
             partner,
@@ -1256,7 +1270,7 @@
         return remote(
             partial.at[j, owner * 2 + core],
             ring_in.at[j, d, owner],
-            send_z.at[d, step],
+            send_z,
             recv_z.at[j, d, step],
             q,
             beside(d),
@@ -1301,14 +1315,8 @@
             back_leg(j).start()
 
     def sums_left():
-        for j in range(groups_ep):
-            took(pair_in.at[j], send_p.at[j])
-        for d in range(2):
-            far = z if d == 0 else chips - 1 - z
-            for step in range(steps):
-                pl.when(far <= step)(
-                    lambda d=d, step=step: took(partial.at[:, 0], send_z.at[d, step])
-                )
+        took(pair_in, send_p)
+        took(pair_in.at[:, pl.ds(0, steps)], send_z)
         took(back_in, send_b)
 
     def routed_stage():
@@ -1338,90 +1346,90 @@
 
     steps = chips - 1
     rows_start()
+    passes(0, 0)
+    passes(1, 0)
     rows_here(0)
+    norm_stage()
     rows_beside(0)
     rows_here(1)
-    rows_far(0)
-    passes(0, 0)
+    rows_here(2)
     rows_beside(1)
-    rows_here(2)
-    passes(1, 0)
     rows_here(3)
-    norm_stage()
     pick_stage(0)
-    own_legs(1)
+    own_legs(0)
     rows_beside(2)
     up_stage(0, 0)
+    rows_far(1)
     up_stage(0, 1)
     rows_beside(3)
     takes(0, 0)
     down_stage(0)
     pick_stage(1)
-    rows_far(1)
     up_stage(1, 0)
     send_sums(0, 0)
-    rows_far(2)
     up_stage(1, 1)
+    rows_far(3)
     down_stage(1)
-    send_sums(0, 1)
     takes(0, 1)
     pick_stage(2)
+    send_sums(0, 1)
+    rows_far(0)
     send_sums(1, 0)
+    send_sums(1, 1)
+    up_stage(2, 0)
+    rows_far(2)
     takes(1, 0)
-    up_stage(2, 0)
     up_stage(2, 1)
     down_stage(2)
+    pick_stage(3)
+    relays(0, 0)
+    send_sums(0, 2)
     send_sums(2, 0)
-    rows_far(3)
-    send_sums(0, 2)
-    send_sums(2, 1)
-    relays(0, 0)
-    pick_stage(3)
     up_stage(3, 0)
     up_stage(3, 1)
+    send_sums(2, 1)
+    takes(0, 2)
     down_stage(3)
-    send_sums(2, 2)
-    takes(0, 2)
+    shares_on(1, 0)
+    own_legs(1)
+    relays(0, 1)
     send_sums(3, 0)
-    send_sums(1, 1)
+    relays(0, 2)
+    takes(1, 1)
     send_sums(3, 1)
-    relays(0, 1)
-    own_legs(0)
-    relays(0, 2)
-    shares_on(1, 0)
-    takes(1, 1)
+    glu_stage(0)
     shares_on(0, 0)
+    send_sums(3, 2)
+    own_sums(0)
     send_sums(1, 2)
-    glu_stage(0)
-    own_sums(0)
     shares_on(0, 1)
-    send_sums(3, 2)
     glu_stage(1)
     shares_on(0, 2)
     takes(1, 2)
+    send_sums(2, 2)
+    own_sums(3)
     glu_stage(3)
+    glu_stage(2)
+    own_sums(1)
+    conv_stage(3)
+    shares_on(1, 1)
+    conv_stage(1)
     own_sums(2)
-    glu_stage(2)
-    halo_start()
-    shares_on(1, 1)
-    own_sums(1)
-    own_sums(3)
-    conv_start()
+    conv_stage(0)
     conv_stage(2)
     shares_on(1, 2)
-    conv_stage(0)
-    conv_stage(3)
-    conv_stage(1)
-    act_stage()
-    out_stage(1)
+    act_tail()
+    conv_head()
+    act_head()
+    out_stage(0)
     out_stage(2)
     out_stage(3)
-    out_stage(0)
+    out_stage(1)
     routed_stage()
 
     rows_left()
     shares_left()
-    pl.when(me < devices - 1)(lambda: halo().wait_send())
+    pl.when(me < devices - 1)(lambda: took(tail_out, send_h))
     sums_left()
     for m in range(chips):
         projected_out(m).wait()
@@ -1554,13 +1562,13 @@
             dma((groups_ep,)),
             dma((2, chips - 1)),
             dma((2, 2, chips - 1)),
-            dma((2, chips - 1)),
+            dma,
             dma((2, 2, 2, chips - 1)),
-            dma((2, chips)),
+            dma((3,)),
             dma((2, 2, chips)),
+            dma,
             dma((groups_ep,)),
-            dma((groups_ep,)),
-            dma((2, chips - 1)),
+            dma,
             dma((groups_ep, 2, chips - 1)),
             dma,
             dma,

time: 77.6 us -> 73.7 us (0.950)
  the two profiles are of different devices: /device:TPU:4 before, /device:TPU:0 now
where the time goes in v4:
time: 73.7 us; the launch traced here: 73.5 us
  Pallas kernels  72.6 us (99%)
  between operations  0.8 us (1%)
    pallas_call x1, Pallas kernels, fused(): pl.pallas_call(functools.partial(fused_kernel, groups_ep, groups_tp, capa...  70.1 us
    pallas_call x1, Pallas kernels, fused(): pl.pallas_call(finish_kernel, out_shape=[jax.ShapeDtypeStruct(mixer_in.sh...  2.53 us

profile of v4, /device:TPU:0, one launch (start us, length us, event | category | flops | bytes accessed | tf_op | source)
XLA Modules:
  0.0 73.5 jit_solution(8475600060599719988)
XLA Ops:
  0.6 70.1 %shard_map.167 = (f32[256,2048]{1,0:T(8,128)}, bf16[32,2048]{1,0:T(8,128)(2,1)}) custom-call(bf16[32,2048]{1,0:T(8,128)(2,1)} %expert_in_hbm.1, f32[1,2048]{1,0:T(1,128)} %bitcast.7, s32[2,32]{1,0:T(2,128)} %bitcast.12, f32[2,32]{1,0:T(2,128)} %bitcast.13, f32[1,2048]{1,0:T(1,128)} %bitcast.8, bf16[256,2048]{1,0:T(8,128)(2,1)} %mixer_hbm.1, ...), custom_call_target="tpu_custom_call" | custom-call | tf_op jit(solution)/shard_map/pallas_call | solution.py:1513
  70.8 2.5 %shard_map.168 = (bf16[256,2048]{1,0:T(8,128)(2,1)}, bf16[32,2048]{1,0:T(8,128)(2,1)}) custom-call(f32[256,2048]{1,0:T(8,128)} %get-tuple-element.4.projected_hbm, bf16[32,2048]{1,0:T(8,128)(2,1)} %get-tuple-element.5.routed_hbm, f32[1,2048]{1,0:T(1,128)} %bitcast.10), custom_call_target="tpu_custom_call" | custom-call | tf_op jit(solution)/shard_map/pallas_call | solution.py:1597
